TPU v7x, 128 devices: a whole 4x4x4 slice. The times are simulated.
128 devices in a mesh: sp: 16 (over z, y), tp: 8 (over x, core).
Axes of the slice: x: 4, y: 4, z: 4, core: 2. Of those that a mesh axis runs over, the one named last changes fastest.
Arguments:
- inputs: bfloat16 [16384, 2048], P(('sp', 'tp')), may hold values from -90 to 90
- in_gain: float32 [2048], replicated, may hold values from 0.1 to 1.9
- w_query: bfloat16 [2048, 1024], replicated, may hold values from -2 to 2
- w_key: bfloat16 [2048, 128], replicated, may hold values from -2 to 2
- w_value: bfloat16 [2048, 128], replicated, may hold values from -0.125 to 0.125
- query_gain: float32 [64], replicated, may hold values from 0 to 8, as said below
- key_gain: float32 [64], replicated, may hold values from 0 to 8, as said below
- decay_sums: float32 [16384, 16], P('sp', 'tp'), may hold values from -2343 to 0, as said below
- w_out: bfloat16 [1024, 2048], replicated, may hold values from -0.1875 to 0.1875
Outputs:
- result: bfloat16 [16384, 2048], P(('sp', 'tp'))
Inputs may be any that keep to these rules, and one draw needn't show every extreme that they name: `decay_sums`: along positions, each head's entries never rise. `query_gain`: every entry is positive. `key_gain`: every entry is positive.
All inputs are finite; a program needn't handle non-finite values.
Results may differ from a plain program's by a relative error of at most 0.015.
The roundings to bfloat16 on the way count: a program that leaves them out, or rounds other values in their place, can miss the bound.
Values may be sent and summed in bfloat16 or wider, within the bound.
A program may use at most 64 MiB of HBM per device.

v0:
```python
from functools import partial
import math

import jax
import jax.numpy as jnp
from jax import lax
from jax.sharding import Mesh
from jax.sharding import PartitionSpec as P

TP = ("tp_0", "tp_1")
SP_TP = ("sp", "tp_0", "tp_1")


epsilon = 1e-06


def joined_along(tiles, dim):
    tiles = jnp.moveaxis(tiles, 0, dim)
    lengths = tiles.shape
    return tiles.reshape(*lengths[:dim], lengths[dim] * lengths[dim + 1], *lengths[dim + 2 :])


def from_everyone(value, axis):
    length = lax.axis_size(axis)
    return lax.all_to_all(
        jnp.broadcast_to(value[None], (length, *value.shape)), axis, 0, 0, tiled=True
    )


def gathered_copies(value, axis, dim):
    return joined_along(from_everyone(value, axis), dim)


def partner(value, axis, stride):
    return lax.ppermute(value, axis, [(i, i ^ 1 << stride) for i in range(lax.axis_size(axis))])


def cut_along(value, dim, length):
    before, after = (value.shape[:dim], value.shape[dim + 1 :])
    return jnp.moveaxis(value.reshape(*before, length, -1, *after), dim, 0)


def moved_by_axis(tiles, axes, sequence):
    inside = tiles.shape[1:]
    filled = tiles.reshape(*(lax.axis_size(a) for a in axes), *inside)
    for k in sequence:
        filled = lax.all_to_all(filled, axes[k], k, k, tiled=True)
    return filled.reshape(-1, *inside)


def stepwise_exchange(value, axes, sequence, split_dim, concat_dim):
    tiles = cut_along(value, split_dim, lax.axis_size(axes))
    return joined_along(moved_by_axis(tiles, axes, sequence), concat_dim)


def rms_norm(vector, gain_vec):
    return (
        vector * lax.rsqrt(jnp.mean(vector * vector, axis=-1, keepdims=True) + epsilon) * gain_vec
    )


def attend_step(
    masked, query_rows, query_decay, query_pos, key_slice, value_slice, decay_slice, key_pos, inner
):
    peak, total, weighted = inner
    score_scale = query_rows.shape[2] ** (-0.5)
    scores = (
        jnp.einsum("thd,ud->htu", query_rows, key_slice, preferred_element_type=jnp.float32)
        * score_scale
    )
    scores = scores + query_decay[:, :, None] - decay_slice[:, None, :]
    if masked:
        visible = key_pos[None, :] <= query_pos[:, None]
        scores = jnp.where(visible[None], scores, -1e30)
    peak_new = jnp.maximum(peak, jnp.max(scores, axis=-1))
    weights_exp = jnp.exp(scores - peak_new[:, :, None])
    if masked:
        weights_exp = jnp.where(visible[None], weights_exp, 0.0)
    rescale = jnp.exp(peak - peak_new)
    total_new = total * rescale + jnp.sum(weights_exp, axis=-1)
    product = jnp.einsum(
        "htu,ud->thd",
        weights_exp.astype(jnp.bfloat16),
        value_slice,
        preferred_element_type=jnp.float32,
    )
    weighted_new = weighted * rescale.T[:, :, None] + product
    return (peak_new, total_new, weighted_new)


def keep_state(inner):
    return inner


def per_device(inputs, in_gain, w_query, w_key, w_value, query_gain, key_gain, decay_sums, w_out):
    tp_count = lax.axis_size(TP)
    sp_count = lax.axis_size("sp")
    sp_rank = lax.axis_index("sp")
    heads_dev = decay_sums.shape[1]
    head_size = query_gain.shape[0]
    kv_heads = w_key.shape[1] // head_size
    width_dev = heads_dev * head_size
    normed = rms_norm(inputs.astype(jnp.float32), in_gain).astype(jnp.bfloat16)
    row_count = normed.shape[0]
    all_heads = w_query.shape[1] // head_size
    query_all = rms_norm(
        jnp.dot(normed, w_query, preferred_element_type=jnp.float32).reshape(
            row_count, all_heads, head_size
        ),
        query_gain,
    ).astype(jnp.bfloat16)
    key_all = rms_norm(
        jnp.dot(normed, w_key, preferred_element_type=jnp.float32).reshape(
            row_count, kv_heads, head_size
        ),
        key_gain,
    ).astype(jnp.bfloat16)
    value_all = (
        jnp.dot(normed, w_value, preferred_element_type=jnp.float32)
        .astype(jnp.bfloat16)
        .reshape(row_count, kv_heads, head_size)
    )
    pair_all = jnp.repeat(
        jnp.concatenate([key_all, value_all], axis=2), tp_count // kv_heads, axis=1
    )
    packed = jnp.concatenate([query_all.reshape(row_count, tp_count, width_dev), pair_all], axis=2)
    received = lax.all_to_all(packed, TP, split_axis=1, concat_axis=0, tiled=True)[:, 0]
    tok_rows = received.shape[0]
    queries = received[:, :width_dev].reshape(tok_rows, heads_dev, head_size)
    key_values = received[:, width_dev:]
    all_decays = gathered_copies(decay_sums, "sp", 0)
    half_rows = tok_rows // 2
    bit_steps = sp_count.bit_length() - 1
    far_queries = queries[half_rows:]
    for bit in range(bit_steps):
        far_queries = partner(far_queries, "sp", bit)
    mirror = sp_count - 1 - sp_rank
    groups = [
        (queries[:half_rows], sp_rank * tok_rows),
        (far_queries, mirror * tok_rows + half_rows),
    ]
    prepared = []
    for query_rows, first_pos in groups:
        rows = query_rows.shape[0]
        query_decay = lax.dynamic_slice_in_dim(all_decays, first_pos, rows, 0).T
        query_pos = first_pos + jnp.arange(rows, dtype=jnp.int32)
        prepared.append((query_rows, query_decay, query_pos, first_pos, first_pos + rows - 1))
    initial = tuple(
        (
            (
                jnp.full((heads_dev, entry[0].shape[0]), -1e30, jnp.float32),
                jnp.zeros((heads_dev, entry[0].shape[0]), jnp.float32),
                jnp.zeros((entry[0].shape[0], heads_dev, head_size), jnp.float32),
            )
            for entry in prepared
        )
    )
    state = initial
    pieces = lax.all_gather(key_values, "sp", axis=0, tiled=True)
    piece_rows = pieces.shape[0]
    key_block = math.gcd(piece_rows, 512)

    def one_block(carry, block_index):
        key_start = block_index * key_block
        pair_slice = lax.dynamic_slice_in_dim(pieces, block_index * key_block, key_block, 0)
        key_slice = pair_slice[:, :head_size]
        value_slice = pair_slice[:, head_size:]
        decay_slice = lax.dynamic_slice_in_dim(all_decays, key_start, key_block, 0).T
        key_pos = key_start + jnp.arange(key_block, dtype=jnp.int32)
        updated = []
        for (query_rows, query_decay, query_pos, first_pos, last_pos), inner in zip(
            prepared, carry
        ):
            branch = jnp.where(
                key_start > last_pos, 0, jnp.where(key_start + key_block - 1 <= first_pos, 1, 2)
            )
            full_step = partial(
                attend_step,
                False,
                query_rows,
                query_decay,
                query_pos,
                key_slice,
                value_slice,
                decay_slice,
                key_pos,
            )
            masked_step = partial(
                attend_step,
                True,
                query_rows,
                query_decay,
                query_pos,
                key_slice,
                value_slice,
                decay_slice,
                key_pos,
            )
            updated.append(lax.switch(branch, [keep_state, full_step, masked_step], inner))
        return (tuple(updated), None)

    state, unused = lax.scan(one_block, state, jnp.arange(piece_rows // key_block, dtype=jnp.int32))
    outputs = [
        (weighted / total.T[:, :, None]).astype(jnp.bfloat16) for peak, total, weighted in state
    ]
    returned = outputs[1]
    for bit in range(bit_steps):
        returned = partner(returned, "sp", bit)
    attended = jnp.concatenate([outputs[0], returned], axis=0).reshape(tok_rows, width_dev)
    out_rows = stepwise_exchange(attended, TP, (1, 0), 0, 1)
    result = jnp.dot(out_rows, w_out, preferred_element_type=jnp.float32).astype(jnp.bfloat16)
    return result


def solution(mesh):
    torus = Mesh(mesh.devices.reshape(mesh.shape["sp"], 4, 2), ("sp", "tp_0", "tp_1"))
    in_specs = (P(SP_TP, None), P(), P(), P(), P(), P(), P(), P("sp", TP), P())
    out_specs = P(SP_TP, None)
    return jax.shard_map(
        per_device, mesh=torus, in_specs=in_specs, out_specs=out_specs, check_vma=False
    )
```

profile of v0, /device:TPU:33, one launch (start us, length us, event | category | flops | bytes accessed | tf_op | source)
XLA Modules:
  0.0 264.8 jit_solution(12323590933669240431)
XLA Ops:
  7.9 1.5 multiply_reduce_fusion
  9.4 1.6 convolution_convert_fusion.1
  11.0 3.0 %fusion.64 = (f32[128,1024]{1,0:T(8,128)S(1)}, f32[128,1024]{1,0:T(8,128)S(1)}) fusion(bf16[2048,1024]{1,0:T(8,128)(2,1)} %param.19, bf16[128,2048]{1,0:T(8,128)(2,1)S(1)} %copy-done.1, f32[2048]{0:T(1024)S(1)} %copy-done.2, f32[128]{0:T(128)S(1)} %add_rsqrt_fusion.2), kind=kOutput, calls=%fused_computation.100 | convolution fusion | flops 538050560 | bytes 5775872 | tf_op jit(solution)/shard_map/dot_general | solution.py:107
  15.1 14.1 %all_to_all.30 = bf16[128,8,256]{0,2,1:T(8,128)(2,1)S(1)} all-to-all(bf16[128,8,256]{0,2,1:T(8,128)(2,1)S(1)} %pad_maximum_fusion), channel_id=1, replica_groups=mesh['sp'=16,'tp_0'=4,'tp_1'=2] {'tp_0','tp_1'}, dimensions={1} | all-to-all | bytes 1048576 | tf_op jit(solution)/shard_map/all_to_all | solution.py:127
  31.7 2.5 collective-permute-done
  34.2 2.9 %collective-permute-start.1 = (bf16[512,2,64]{0,2,1:T(8,128)(2,1)S(1)}, bf16[512,2,64]{0,2,1:T(8,128)(2,1)S(1)}, u32[]{:S(2)}, u32[]{:S(2)}) collective-permute-start(bf16[512,2,64]{0,2,1:T(8,128)(2,1)S(1)} %collective-permute-done), channel_id=1, source_target_pairs={{0,16},{8,24},{16,0},{24,8},{32,48},{40,56},{48,32},{56,40},{64,80... | collective-permute-start | bytes 393224 | tf_op jit(solution)/shard_map/ppermute | solution.py:35
  37.1 2.4 collective-permute-done.1
  40.2 8.6 %all-to-all-start.1 = ((f32[16,1024,2]{1,2,0:T(2,128)}), f32[16,1024,2]{1,2,0:T(2,128)S(1)}, u32[]{:S(2)}, u32[]{:S(2)}) async-start(f32[16,1024,2]{1,2,0:T(2,128)} %broadcast_in_dim.53), calls=%async_computation.1 | async-start | bytes 262144 | tf_op jit(solution)/shard_map/all_to_all | solution.py:25
  48.9 1.9 collective-permute-start.3
  50.8 3.7 %all-to-all-done.1 = f32[16,1024,2]{1,2,0:T(2,128)S(1)} async-done(((f32[16,1024,2]{1,2,0:T(2,128)}), f32[16,1024,2]{1,2,0:T(2,128)S(1)}, u32[]{:S(2)}, u32[]{:S(2)}) %all-to-all-start.1) | async-done | bytes 131104 | tf_op jit(solution)/shard_map/all_to_all | solution.py:25
  55.2 28.2 %all-gather.2.cloned.1.call-done = bf16[16384,128]{1,0:T(8,128)(2,1)} async-done(((bf16[1024,128]{1,0:T(8,128)(2,1)}), bf16[16384,128]{1,0:T(8,128)(2,1)}) %all-gather.2.cloned.1.call-update) | async-done | bytes 4194320 | tf_op jit(solution)/shard_map/all_gather | solution.py:159
  83.6 133.3 %while.26 = (s32[]{:T(128)}, f32[2,512]{1,0:T(2,128)S(1)}, f32[2,512]{1,0:T(2,128)S(1)}, f32[512,2,64]{0,2,1:T(8,128)S(1)}, f32[2,512]{1,0:T(2,128)S(1)}, /*inde...) while((s32[]{:T(128)}, f32[2,512]{1,0:T(2,128)S(1)}, ...), condition=%wide.region_18.19_spmd.clone.clone, body=%wide.region_3.18_spmd.clone.clone.sunk | while | flops 280763904 | bytes 16956256 | solution.py:202
  87.6 1.4 conditional.8
  91.6 1.4 conditional.9
  93.1 1.4 conditional.8
  98.5 1.4 conditional.8
  104.0 1.4 conditional.8
  109.4 1.4 conditional.8
  114.9 1.4 conditional.8
  120.3 1.4 conditional.8
  124.4 1.4 conditional.9
  125.8 1.4 conditional.8
  129.8 1.4 conditional.9
  131.3 2.1 conditional.8
  136.0 1.4 conditional.9
  140.1 1.4 conditional.9
  144.2 1.4 conditional.9
  148.3 1.4 conditional.9
  152.3 1.4 conditional.9
  156.4 1.4 conditional.9
  160.5 1.4 conditional.9
  164.6 1.4 conditional.9
  168.6 1.4 conditional.9
  172.7 1.4 conditional.9
  176.8 1.4 conditional.9
  180.9 1.4 conditional.9
  184.9 1.4 conditional.9
  189.0 1.4 conditional.9
  193.1 2.1 conditional.9
  217.0 4.2 %collective-permute-done.4 = bf16[512,2,64]{0,2,1:T(8,128)(2,1)S(1)} collective-permute-done((bf16[512,2,64]{0,2,1:T(8,128)(2,1)S(1)}, bf16[512,2,64]{0,2,1:T(8,128)(2,1)S(1)}, u32[]{:S(2)}, u32[]{:S(2)}) %collective-permute-start.4) | collective-permute-done | bytes 131104 | tf_op jit(solution)/shard_map/ppermute | solution.py:35
  221.2 1.6 collective-permute-start.5
  222.8 3.8 %collective-permute-done.5 = bf16[512,2,64]{0,2,1:T(8,128)(2,1)S(1)} collective-permute-done((bf16[512,2,64]{0,2,1:T(8,128)(2,1)S(1)}, bf16[512,2,64]{0,2,1:T(8,128)(2,1)S(1)}, u32[]{:S(2)}, u32[]{:S(2)}) %collective-permute-start.5) | collective-permute-done | bytes 131104 | tf_op jit(solution)/shard_map/ppermute | solution.py:35
  226.9 3.4 %collective-permute-done.6 = bf16[512,2,64]{0,2,1:T(8,128)(2,1)S(1)} collective-permute-done((bf16[512,2,64]{0,2,1:T(8,128)(2,1)S(1)}, bf16[512,2,64]{0,2,1:T(8,128)(2,1)S(1)}, u32[]{:S(2)}, u32[]{:S(2)}) %collective-permute-start.6) | collective-permute-done | bytes 131104 | tf_op jit(solution)/shard_map/ppermute | solution.py:35
  230.3 2.0 collective-permute-start.7
  232.3 3.7 %collective-permute-done.7 = bf16[512,2,64]{0,2,1:T(8,128)(2,1)S(1)} collective-permute-done((bf16[512,2,64]{0,2,1:T(8,128)(2,1)S(1)}, bf16[512,2,64]{0,2,1:T(8,128)(2,1)S(1)}, u32[]{:S(2)}, u32[]{:S(2)}) %collective-permute-start.7) | collective-permute-done | bytes 131104 | tf_op jit(solution)/shard_map/ppermute | solution.py:35
  236.3 8.3 %all_to_all.31 = bf16[4,2,128,128]{2,3,0,1:T(8,128)(2,1)S(1)} all-to-all(bf16[4,2,128,128]{2,3,0,1:T(8,128)(2,1)S(1)} %copy.78), channel_id=1, replica_groups=mesh['sp'=16,'tp_0'=4,'tp_1'=2] {'tp_1'}, dimensions={1} | all-to-all | bytes 524288 | tf_op jit(solution)/shard_map/all_to_all | solution.py:47
  244.7 9.6 %all_to_all.32 = bf16[4,2,128,128]{2,3,1,0:T(8,128)(2,1)S(1)} all-to-all(bf16[4,2,128,128]{2,3,1,0:T(8,128)(2,1)S(1)} %copy.79), channel_id=1, replica_groups=mesh['sp'=16,'tp_0'=4,'tp_1'=2] {'tp_0'}, dimensions={0} | all-to-all | bytes 524288 | tf_op jit(solution)/shard_map/all_to_all | solution.py:47
  254.3 3.7 %convolution_convert_fusion = bf16[128,2048]{1,0:T(8,128)(2,1)} fusion(bf16[128,1024]{0,1:T(8,128)(2,1)S(1)} %bitcast.133, bf16[1024,2048]{1,0:T(8,128)(2,1)} %param.25), kind=kOutput, calls=%fused_computation.69 | convolution fusion | flops 537133056 | bytes 4980736 | tf_op jit(solution)/shard_map/dot_general | solution.py:211
  (550 shorter events, 122.1 us)
Async XLA Ops:
  6.5 1.3 copy-start
  6.5 4.4 %copy-start.1 = (bf16[128,2048]{1,0:T(8,128)(2,1)S(1)}, bf16[128,2048]{1,0:T(8,128)(2,1)}, u32[]{:S(2)}) copy-start(bf16[128,2048]{1,0:T(8,128)(2,1)} %param.17) | copy-start | bytes 1572868
  6.5 4.5 %copy-start.2 = (f32[2048]{0:T(1024)S(1)}, f32[2048]{0:T(1024)}, u32[]{:S(2)}) copy-start(f32[2048]{0:T(1024)} %param.18) | copy-start | bytes 24580
  6.5 76.9 %all-gather.2.cloned.1.call-start = ((), (), s32[]{:S(2)}) async-start(), calls=%async_computation.4 | async-start | bytes 4456448 | tf_op jit(solution)/shard_map/all_gather | solution.py:159
  14.0 0.7 copy-start.5
  14.0 0.7 copy-start.4
  15.1 24.5 %copy-start.3 = (f32[1024,2]{0,1:T(2,128)S(1)}, f32[1024,2]{0,1:T(2,128)}, u32[]{:S(2)}) copy-start(f32[1024,2]{0,1:T(2,128)} %param.24) | copy-start | bytes 24580
  30.3 3.9 %collective-permute-start = (bf16[512,2,64]{0,2,1:T(8,128)(2,1)S(1)}, bf16[512,2,64]{0,2,1:T(8,128)(2,1)S(1)}, u32[]{:S(2)}, u32[]{:S(2)}) collective-permute-start(bf16[512,2,64]{0,2,1:T(8,128)(2,1)S(1)} %bitcast.139), channel_id=1, source_target_pairs={{0,8},{8,0},{16,24},{24,16},{32,40},{40,32},{48,56},{56,48},{64,72... | collective-permute-start | bytes 393224 | tf_op jit(solution)/shard_map/ppermute | solution.py:35
  34.2 5.4 %collective-permute-start.1 = (bf16[512,2,64]{0,2,1:T(8,128)(2,1)S(1)}, bf16[512,2,64]{0,2,1:T(8,128)(2,1)S(1)}, u32[]{:S(2)}, u32[]{:S(2)}) collective-permute-start(bf16[512,2,64]{0,2,1:T(8,128)(2,1)S(1)} %collective-permute-done), channel_id=1, source_target_pairs={{0,16},{8,24},{16,0},{24,8},{32,48},{40,56},{48,32},{56,40},{64,80... | collective-permute-start | bytes 393224 | tf_op jit(solution)/shard_map/ppermute | solution.py:35
  39.5 9.3 %collective-permute-start.2 = (bf16[512,2,64]{0,2,1:T(8,128)(2,1)S(1)}, bf16[512,2,64]{0,2,1:T(8,128)(2,1)S(1)}, u32[]{:S(2)}, u32[]{:S(2)}) collective-permute-start(bf16[512,2,64]{0,2,1:T(8,128)(2,1)S(1)} %collective-permute-done.1), channel_id=1, source_target_pairs={{0,32},{8,40},{16,48},{24,56},{32,0},{40,8},{48,16},{56,24},{64,96... | collective-permute-start | bytes 393224 | tf_op jit(solution)/shard_map/ppermute | solution.py:35
  40.2 14.2 %all-to-all-start.1 = ((f32[16,1024,2]{1,2,0:T(2,128)}), f32[16,1024,2]{1,2,0:T(2,128)S(1)}, u32[]{:S(2)}, u32[]{:S(2)}) async-start(f32[16,1024,2]{1,2,0:T(2,128)} %broadcast_in_dim.53), calls=%async_computation.1 | async-start | bytes 262144 | tf_op jit(solution)/shard_map/all_to_all | solution.py:25
  48.9 6.3 %collective-permute-start.3 = (bf16[512,2,64]{0,2,1:T(8,128)(2,1)S(1)}, bf16[512,2,64]{0,2,1:T(8,128)(2,1)S(1)}, u32[]{:S(2)}, u32[]{:S(2)}) collective-permute-start(bf16[512,2,64]{0,2,1:T(8,128)(2,1)S(1)} %collective-permute-done.2), channel_id=1, source_target_pairs={{0,64},{8,72},{16,80},{24,88},{32,96},{40,104},{48,112},{56,120},{... | collective-permute-start | bytes 393224 | tf_op jit(solution)/shard_map/ppermute | solution.py:35
  216.9 4.3 %collective-permute-start.4 = (bf16[512,2,64]{0,2,1:T(8,128)(2,1)S(1)}, bf16[512,2,64]{0,2,1:T(8,128)(2,1)S(1)}, u32[]{:S(2)}, u32[]{:S(2)}) collective-permute-start(bf16[512,2,64]{0,2,1:T(8,128)(2,1)S(1)} %divide_convert_fusion), channel_id=1, source_target_pairs={{0,8},{8,0},{16,24},{24,16},{32,40},{40,32},{48,56},{56,48},{64,72... | collective-permute-start | bytes 393224 | tf_op jit(solution)/shard_map/ppermute | solution.py:35
  221.2 5.3 %collective-permute-start.5 = (bf16[512,2,64]{0,2,1:T(8,128)(2,1)S(1)}, bf16[512,2,64]{0,2,1:T(8,128)(2,1)S(1)}, u32[]{:S(2)}, u32[]{:S(2)}) collective-permute-start(bf16[512,2,64]{0,2,1:T(8,128)(2,1)S(1)} %collective-permute-done.4), channel_id=1, source_target_pairs={{0,16},{8,24},{16,0},{24,8},{32,48},{40,56},{48,32},{56,40},{64,80... | collective-permute-start | bytes 393224 | tf_op jit(solution)/shard_map/ppermute | solution.py:35
  226.5 3.8 %collective-permute-start.6 = (bf16[512,2,64]{0,2,1:T(8,128)(2,1)S(1)}, bf16[512,2,64]{0,2,1:T(8,128)(2,1)S(1)}, u32[]{:S(2)}, u32[]{:S(2)}) collective-permute-start(bf16[512,2,64]{0,2,1:T(8,128)(2,1)S(1)} %collective-permute-done.5), channel_id=1, source_target_pairs={{0,32},{8,40},{16,48},{24,56},{32,0},{40,8},{48,16},{56,24},{64,96... | collective-permute-start | bytes 393224 | tf_op jit(solution)/shard_map/ppermute | solution.py:35
  230.3 5.7 %collective-permute-start.7 = (bf16[512,2,64]{0,2,1:T(8,128)(2,1)S(1)}, bf16[512,2,64]{0,2,1:T(8,128)(2,1)S(1)}, u32[]{:S(2)}, u32[]{:S(2)}) collective-permute-start(bf16[512,2,64]{0,2,1:T(8,128)(2,1)S(1)} %collective-permute-done.6), channel_id=1, source_target_pairs={{0,64},{8,72},{16,80},{24,88},{32,96},{40,104},{48,112},{56,120},{... | collective-permute-start | bytes 393224 | tf_op jit(solution)/shard_map/ppermute | solution.py:35
Sparse Core Ops, SparseCore 0:
  30.3 53.1 all-gather.1
where the time goes:
time: 269 us; the launch traced here: 265 us
  local copies, waits for them, and re-layouts  63.6 us (24%)
  waiting for transfers between devices  52.6 us (20%)
  matrix products  43.4 us (16%)
  blocking collectives  32 us (12%)
  loops' own time  27.2 us (10%)
  starting transfers between devices  18.8 us (7%)
  between operations  13.7 us (5%)
  other arithmetic  13.4 us (5%)
    slice x32, local copies, waits for them, and re-layouts, one_block(): value_slice = pair_slice[:, head_size:]  35.1 us
    all_gather x1, waiting for transfers between devices, per_device(): pieces = lax.all_gather(key_values, 'sp', axis=0, tiled=True)  28.2 us
    another operation x1, loops' own time, per_device(): lax.scan(one_block, state, jnp.arange(piece_rows // key_block, dtype=jnp....  24.6 us
    ppermute x8, waiting for transfers between devices, partner(): lax.ppermute(value, axis, [(i, i ^ 1 << stride) for i in range(lax.axis_s...  20.7 us
    dynamic_slice x32, local copies, waits for them, and re-layouts, per_device(): lax.scan(one_block, state, jnp.arange(piece_rows // key_block, dtype=jnp....  18.8 us
    all_to_all x2, blocking collectives, moved_by_axis(): filled = lax.all_to_all(filled, axes[k], k, k, tiled=True)  17.9 us
    dot_general x33, matrix products, attend_step(): jnp.einsum('htu,ud->thd', weights_exp.astype(jnp.bfloat16), value_slice,...  17.1 us
    dot_general x33, matrix products, attend_step(): jnp.einsum('thd,ud->htu', query_rows, key_slice, preferred_element_type=j...  16.6 us
  transfers between devices with their start and end apart: 10, of which 9 were waited for; matrix products, arithmetic and copies ran while one was open for 0% of the time, Pallas kernels for 0%

commit v1 on v0

v1 whole, which is shorter than its diff:
```python
import functools

import jax
import jax.numpy as jnp
from jax import lax
from jax.experimental import pallas as pl
from jax.experimental.pallas import tpu as pltpu
from jax.sharding import Mesh
from jax.sharding import PartitionSpec as P

f32 = jnp.float32
bf = jnp.bfloat16
LOG2E = 1.4426950408889634
EPS = 1e-06
MESH = pl.DeviceIdType.MESH
VM = pl.BlockSpec(memory_space=pltpu.VMEM)


def split3(x):
    high = x.astype(bf).astype(f32)
    rest = x - high
    mid = rest.astype(bf).astype(f32)
    return high, mid, rest - mid


def head_norm(flat, heads, gain):
    x = flat.reshape(heads, 64, flat.shape[1])
    scale = lax.rsqrt(jnp.mean(x * x, axis=1, keepdims=True) + EPS)
    return (x * scale * gain[None]).reshape(flat.shape)


def project_kernel(x_ref, gain_ref, wk_ref, wv_ref, wq_ref, qg_ref, kg_ref, q_ref, kv_ref, norm_ref):
    step = pl.program_id(0)

    @pl.when(step == 0)
    def _():
        x = x_ref[...].astype(f32)
        scale = lax.rsqrt(jnp.mean(x * x, axis=1, keepdims=True) + EPS)
        norm_ref[...] = (x * scale * gain_ref[...]).astype(bf)
        keys = jnp.dot(norm_ref[...], wk_ref[...], preferred_element_type=f32)
        values = jnp.dot(norm_ref[...], wv_ref[...], preferred_element_type=f32)
        keys = head_norm(keys.T, 2, kg_ref[...]).astype(bf)
        values = values.T.astype(bf)
        for g in range(2):
            kv_ref[g, 0:64] = keys[g * 64 : (g + 1) * 64]
            kv_ref[g, 64:128] = values[g * 64 : (g + 1) * 64]

    queries = jnp.dot(norm_ref[...], wq_ref[...], preferred_element_type=f32)
    queries = head_norm(queries.T, wq_ref.shape[1] // 64, qg_ref[...])
    q_ref[...] = (queries * (LOG2E / 8)).astype(bf)


def project(x, gain, wk, wv, wq, qg, kg):
    cols = 256
    whole = lambda shape: pl.BlockSpec(shape, lambda j: (0,) * len(shape))
    return pl.pallas_call(
        project_kernel,
        grid=(1024 // cols,),
        out_shape=[jax.ShapeDtypeStruct((1024, 128), bf), jax.ShapeDtypeStruct((2, 128, 128), bf)],
        in_specs=[
            whole((128, 2048)),
            whole((1, 2048)),
            whole((2048, 128)),
            whole((2048, 128)),
            pl.BlockSpec((2048, cols), lambda j: (0, j)),
            whole((64, 1)),
            whole((64, 1)),
        ],
        out_specs=[pl.BlockSpec((cols, 128), lambda j: (j, 0)), whole((2, 128, 128))],
        scratch_shapes=[pltpu.VMEM((128, 2048), bf)],
        compiler_params=pltpu.CompilerParams(vmem_limit_bytes=24 * 1024 * 1024),
        cost_estimate=pl.CostEstimate(
            flops=2 * 128 * 2048 * 1280, bytes_accessed=6 * 1024 * 1024, transcendentals=0
        ),
        name="project",
    )(x, gain, wk, wv, wq, qg, kg)


def line_of(c, a, b):
    a, b = lax.rem(a + 8, 4), lax.rem(b + 8, 4)
    return (1 - c) * (4 * b + a) + c * (4 * a + b)


def gather_kernel(q_ref, kv_ref, d_ref, part_ref, all_ref, dec_ref, *sems):
    ks_send, ks_recv, ds_send, ds_recv, q_send, q_recv, r_send, r_recv, s_send, s_recv = sems
    z, y, x, c = (lax.axis_index(n) for n in ("z", "y", "x", "c"))
    g = x // 2
    line = 4 * z + y
    tp = 2 * x + c
    mine = (x - 2 * g) * 2 + c
    mirror = (3 - z, 3 - y, 3 - x, 1 - c)
    a = (1 - c) * y + c * z
    b = (1 - c) * z + c * y

    def at_ab(pa, pb):
        pa, pb = lax.rem(pa + 8, 4), lax.rem(pb + 8, 4)
        return ((1 - c) * pb + c * pa, (1 - c) * pa + c * pb, x, c)

    def in_line(t):
        t = lax.rem(t + 8, 8)
        return (z, y, t // 2, lax.rem(t, 2))

    barrier = pltpu.get_barrier_semaphore()
    peers = [in_line(tp + k) for k in range(1, 8)] + [mirror]
    peers += [at_ab(a + 1, b), at_ab(a - 1, b), at_ab(a, b + 1), at_ab(a, b - 1)]
    for peer in peers:
        pl.semaphore_signal(barrier, inc=1, device_id=peer, device_id_type=MESH)

    all_ref[line, tp, 0:128] = kv_ref[g]
    dec_ref[mine] = d_ref[...]
    pl.semaphore_wait(barrier, len(peers))

    started = []

    def send(src, dst, send_sem, recv_sem, peer):
        copy = pltpu.make_async_remote_copy(
            src_ref=src,
            dst_ref=dst,
            send_sem=send_sem,
            recv_sem=recv_sem,
            device_id=peer,
            device_id_type=MESH,
        )
        copy.start()
        started.append(copy)
        return copy

    decays = []
    for k in range(1, 4):
        t = lax.rem(mine + k, 4)
        peer = (z, y, 2 * g + t // 2, lax.rem(t, 2))
        decays.append(send(d_ref, dec_ref.at[mine], ds_send.at[k], ds_recv.at[k], peer))
    pieces = []
    for k in range(1, 8):
        t = lax.rem(tp + k, 8)
        pieces.append(
            send(
                kv_ref.at[t // 4],
                all_ref.at[line, tp, pl.ds(0, 128)],
                ks_send.at[k],
                ks_recv.at[k],
                in_line(tp + k),
            )
        )
    q_copy = send(q_ref.at[pl.ds((1 - g) * 512, 512)], part_ref, q_send, q_recv, mirror)

    for copy in decays:
        copy.wait_recv()
    row8 = lax.broadcasted_iota(jnp.int32, (8, 128), 0)
    ones = jnp.where(row8 < 3, 1.0, 0.0).astype(f32)
    for p in range(8):
        cols = slice(p * 128, (p + 1) * 128)
        value = jnp.concatenate([dec_ref[q, :, cols] for q in range(4)], axis=0) * LOG2E
        all_ref[line, p, 128:160] = jnp.concatenate([*split3(value), ones], axis=0).astype(bf)
    for copy in pieces:
        copy.wait_recv()

    def block(ln, sub):
        return all_ref.at[ln, pl.ds(4 * c + 2 * sub, 2)]

    def ring_send(ln, sub, slot, peer):
        return send(block(ln, sub), block(ln, sub), r_send.at[slot], r_recv.at[slot], peer)

    sibling = (z, y, x, 1 - c)
    shared = []

    def share(ln, slot):
        half = all_ref.at[ln, pl.ds(4 * c, 4)]
        shared.append(send(half, half, s_send.at[slot], s_recv.at[slot], sibling))

    def ring_start(step, ln, up, down):
        right = [ring_send(ln, sub, step * 6 + sub, up) for sub in range(2)]
        left = [ring_send(ln, sub, step * 6 + 2 + sub, down) for sub in range(2)]
        return right, left

    def ring_relay(step, copies, ln_left, ln_right, up, down):
        right, left = copies
        right[0].wait_recv()
        first = ring_send(ln_left, 0, step * 6 + 4, up)
        left[1].wait_recv()
        second = ring_send(ln_right, 1, step * 6 + 5, down)
        right[1].wait_recv()
        left[0].wait_recv()
        return first, second

    up_a, down_a = at_ab(a + 1, b), at_ab(a - 1, b)
    up_b, down_b = at_ab(a, b + 1), at_ab(a, b - 1)
    own = [line_of(c, a, b), line_of(c, a - 1, b), line_of(c, a + 1, b), line_of(c, a + 2, b)]
    along_a = (0, -1, 1, 2)

    first_copies = ring_start(0, own[0], up_a, down_a)
    second = [ring_start(1, own[0], up_b, down_b)]
    relays = ring_relay(0, first_copies, own[1], own[2], up_a, down_a)
    for j in (1, 2):
        second.append(ring_start(1 + j, own[j], up_b, down_b))
        share(own[j], j)
    for copy in relays:
        copy.wait_recv()
    second.append(ring_start(4, own[3], up_b, down_b))
    share(own[3], 3)
    last = []
    for j in range(4):
        left_line = line_of(c, a + along_a[j], b - 1)
        right_line = line_of(c, a + along_a[j], b + 1)
        last.append(ring_relay(1 + j, second[j], left_line, right_line, up_b, down_b))
        share(left_line, 4 + 3 * j)
        share(right_line, 5 + 3 * j)
    for j in range(4):
        for copy in last[j]:
            copy.wait_recv()
        share(line_of(c, a + along_a[j], b + 2), 6 + 3 * j)
    q_copy.wait_recv()
    for copy in shared:
        copy.wait_recv()
    for copy in started:
        copy.wait_send()


def gather(q, kv, d):
    dma = lambda *n: pltpu.SemaphoreType.DMA(n)
    return pl.pallas_call(
        gather_kernel,
        out_shape=[jax.ShapeDtypeStruct((512, 128), bf), jax.ShapeDtypeStruct((16, 8, 160, 128), bf)],
        in_specs=[VM, VM, VM],
        out_specs=[VM, VM],
        scratch_shapes=[
            pltpu.VMEM((4, 2, 1024), f32),
            dma(8),
            dma(8),
            dma(4),
            dma(4),
            pltpu.SemaphoreType.DMA,
            pltpu.SemaphoreType.DMA,
            dma(30),
            dma(30),
            dma(16),
            dma(16),
        ],
        compiler_params=pltpu.CompilerParams(
            collective_id=0, has_side_effects=True, vmem_limit_bytes=24 * 1024 * 1024
        ),
        name="gather",
    )(q, kv, d)


def load_keys(kvd, piece, ref_d, ones):
    blk = kvd[piece]
    dec = blk[128:160].astype(f32)
    rel = dec[0:8] + dec[8:16] + dec[16:24] - ref_d
    rows = jnp.concatenate([*split3(rel), ones], axis=0).astype(bf)
    full = jnp.concatenate([blk[0:64], rows, jnp.zeros((32, 128), bf)], axis=0)
    return full.T, blk[64:128]


def attend_kernel(bounded, chunk_pieces, tile, q_ref, part_ref, kvd_ref, oo_ref, op_ref, *scratch):
    qa_ref, acc_ref, sum_ref, max_ref = scratch
    z, y, x, c = (lax.axis_index(n) for n in ("z", "y", "x", "c"))
    g = x // 2
    own = (4 * z + y) * 8 + 2 * x + c
    chunk = chunk_pieces * 128
    row8 = lax.broadcasted_iota(jnp.int32, (8, 128), 0)
    ones = jnp.where(row8 < 3, 1.0, 0.0).astype(f32)
    for rg, out_ref in enumerate((oo_ref, op_ref)):
        blk = own if rg == 0 else 127 - own
        dec = kvd_ref[blk, 128:160].astype(f32)
        dec = dec[0:8] + dec[8:16] + dec[16:24]
        ref_d = jnp.broadcast_to(dec[:, 0:1], (8, 128))
        parts = split3(dec - ref_d)
        for h in range(8):
            onehot = jnp.where(row8 == h, -1.0, 0.0).astype(f32)
            mine = jnp.zeros((8, 128), f32)
            for i, part in enumerate(parts):
                mine = jnp.where(row8 == i, part[h : h + 1], mine)
            rows = jnp.concatenate([onehot, onehot, onehot, mine], axis=0).astype(bf)
            if rg == 0:
                first = pl.multiple_of(g * 512 + h * 64, 64)
                query = q_ref[pl.ds(first, 64), :]
            else:
                query = part_ref[h * 64 : (h + 1) * 64, :]
            qa_ref[:, h * 128 : (h + 1) * 128] = jnp.concatenate(
                [query, rows, jnp.zeros((32, 128), bf)], axis=0
            )
        acc_ref[...] = jnp.zeros_like(acc_ref)
        sum_ref[...] = jnp.zeros_like(sum_ref)
        if not bounded:
            max_ref[...] = jnp.full(max_ref.shape, -1e30, f32)

        def attend_chunk(piece, masked):
            loaded = [load_keys(kvd_ref, piece + j, ref_d, ones) for j in range(chunk_pieces)]
            keys = jnp.concatenate([k for k, _ in loaded], axis=0)
            values = jnp.concatenate([v for _, v in loaded], axis=1)
            for n in range(1024 // tile):
                cols = slice(n * tile, (n + 1) * tile)
                scores = jnp.dot(keys, qa_ref[:, cols], preferred_element_type=f32)
                if masked:
                    shape = (chunk, tile)
                    key_pos = piece * 128 + lax.broadcasted_iota(jnp.int32, shape, 0)
                    query_pos = blk * 128 + (lax.broadcasted_iota(jnp.int32, shape, 1) & 127)
                    scores = jnp.where(key_pos <= query_pos, scores, -1e30)
                if bounded:
                    weights = jnp.exp2(scores)
                    sums = jnp.sum(weights.reshape(chunk // 8, 8, tile), axis=0)
                    sum_ref[:, cols] += sums
                    acc_ref[:, cols] += jnp.dot(
                        values, weights.astype(bf), preferred_element_type=f32
                    )
                else:
                    old = max_ref[0:1, cols]
                    new = jnp.maximum(old, jnp.max(scores, axis=0, keepdims=True))
                    keep = jnp.exp2(old - new)
                    weights = jnp.exp2(scores - new)
                    max_ref[:, cols] = jnp.broadcast_to(new, (8, tile))
                    sums = jnp.sum(weights.reshape(chunk // 8, 8, tile), axis=0)
                    sum_ref[:, cols] = sum_ref[:, cols] * keep + sums
                    acc_ref[:, cols] = acc_ref[:, cols] * keep + jnp.dot(
                        values, weights.astype(bf), preferred_element_type=f32
                    )

        full = blk // chunk_pieces

        def body(i, carry):
            attend_chunk(i * chunk_pieces, False)
            return carry

        lax.fori_loop(0, full, body, 0)
        attend_chunk(full * chunk_pieces, True)
        inverse = 1.0 / jnp.sum(sum_ref[...], axis=0, keepdims=True)
        for h in range(8):
            cols = slice(h * 128, (h + 1) * 128)
            out_ref[h * 64 : (h + 1) * 64, :] = (acc_ref[:, cols] * inverse[:, cols]).astype(bf)


def attend(q, part, kvd, bounded):
    chunk_pieces, tile = (8, 512) if bounded else (4, 256)
    return pl.pallas_call(
        functools.partial(attend_kernel, bounded, chunk_pieces, tile),
        out_shape=[jax.ShapeDtypeStruct((512, 128), bf)] * 2,
        in_specs=[VM, VM, VM],
        out_specs=[VM, VM],
        scratch_shapes=[
            pltpu.VMEM((128, 1024), bf),
            pltpu.VMEM((64, 1024), f32),
            pltpu.VMEM((8, 1024), f32),
            pltpu.VMEM((8, 1024), f32),
        ],
        compiler_params=pltpu.CompilerParams(vmem_limit_bytes=32 * 1024 * 1024),
        cost_estimate=pl.CostEstimate(
            flops=4 * 64 * 1024 * 17408, bytes_accessed=6 * 1024 * 1024, transcendentals=0
        ),
        name="attend_bounded" if bounded else "attend_any",
    )(q, part, kvd)


def output_kernel(oo_ref, op_ref, w_ref, out_ref, got_ref, send_sem, recv_sem):
    z, y, x, c = (lax.axis_index(n) for n in ("z", "y", "x", "c"))
    g = x // 2
    mirror = (3 - z, 3 - y, 3 - x, 1 - c)
    barrier = pltpu.get_barrier_semaphore()
    pl.semaphore_signal(barrier, inc=1, device_id=mirror, device_id_type=MESH)
    pl.semaphore_wait(barrier, 1)
    copy = pltpu.make_async_remote_copy(
        src_ref=op_ref,
        dst_ref=got_ref,
        send_sem=send_sem,
        recv_sem=recv_sem,
        device_id=mirror,
        device_id_type=MESH,
    )
    copy.start()
    here = oo_ref[...].T
    near = pl.multiple_of(g * 512, 512)
    far = pl.multiple_of((1 - g) * 512, 512)
    partial = jnp.dot(here, w_ref[pl.ds(near, 512), :], preferred_element_type=f32)
    copy.wait_recv()
    there = got_ref[...].T
    partial += jnp.dot(there, w_ref[pl.ds(far, 512), :], preferred_element_type=f32)
    out_ref[...] = partial.astype(bf)
    copy.wait_send()


def output(oo, op, w):
    return pl.pallas_call(
        output_kernel,
        out_shape=jax.ShapeDtypeStruct((128, 2048), bf),
        in_specs=[VM, VM, VM],
        out_specs=VM,
        scratch_shapes=[
            pltpu.VMEM((512, 128), bf),
            pltpu.SemaphoreType.DMA,
            pltpu.SemaphoreType.DMA,
        ],
        compiler_params=pltpu.CompilerParams(
            collective_id=1, has_side_effects=True, vmem_limit_bytes=24 * 1024 * 1024
        ),
        name="output",
    )(oo, op, w)


def per_device(inputs, in_gain, w_query, w_key, w_value, query_gain, key_gain, decay_sums, w_out):
    queries, kv = project(
        inputs,
        in_gain.reshape(1, -1),
        w_key,
        w_value,
        w_query,
        query_gain.reshape(-1, 1),
        key_gain.reshape(-1, 1),
    )
    part, kvd = gather(queries, kv, decay_sums.T)
    kvd = kvd.reshape(128, 160, 128)
    bound = 8.0 * 1.02 * jnp.max(jnp.abs(query_gain * key_gain))
    own_out, part_out = lax.cond(
        bound <= 64.0,
        lambda *a: attend(*a, True),
        lambda *a: attend(*a, False),
        queries,
        part,
        kvd,
    )
    return output(own_out, part_out, w_out)


def solution(mesh):
    torus = Mesh(mesh.devices.reshape(4, 4, 4, 2), ("z", "y", "x", "c"))
    every = ("z", "y", "x", "c")
    in_specs = (P(every, None), P(), P(), P(), P(), P(), P(), P(("z", "y"), ("x", "c")), P())
    return jax.shard_map(
        per_device, mesh=torus, in_specs=in_specs, out_specs=P(every, None), check_vma=False
    )
```

time: 269 us -> 116 us (0.43)
  the two profiles are of different devices: /device:TPU:33 before, /device:TPU:1 now
where the time goes in v1:
time: 116 us; the launch traced here: 115 us
  Pallas kernels  103 us (89%)
  local copies, waits for them, and re-layouts  10.5 us (9%)
  other arithmetic  1.29 us (1%)
    pallas_call x1, Pallas kernels, attend(): pl.pallas_call(functools.partial(attend_kernel, bounded, chunk_pieces, ti...  53.9 us
    pallas_call x1, Pallas kernels, gather(): pl.pallas_call(gather_kernel, out_shape=[jax.ShapeDtypeStruct((512, 128),...  34.7 us
    pallas_call x1, Pallas kernels, output(): pl.pallas_call(output_kernel, out_shape=jax.ShapeDtypeStruct((128, 2048),...  11.4 us
    unnamed x15, local copies, waits for them, and re-layouts  8.99 us
    pallas_call x1, Pallas kernels, project(): pl.pallas_call(project_kernel, grid=(1024 // cols,), out_shape=[jax.Shape...  2.92 us

profile of v1, /device:TPU:1, one launch (start us, length us, event | category | flops | bytes accessed | tf_op | source)
XLA Modules:
  0.0 115.4 jit_solution(1052618629658306284)
XLA Ops:
  0.0 0.0 copy-start.6
  0.0 1.3 %abs_reduce_fusion = f32[]{:T(128)} fusion(f32[64]{0:T(128)} %param.16, f32[64]{0:T(128)} %param.17), kind=kLoop, calls=%fused_computation | loop fusion | flops 191 | bytes 516 | tf_op jit(solution)/shard_map/reduce_max | solution.py:411
  1.9 0.7 copy.11.kg_ref
  2.7 0.7 copy.10.qg_ref
  3.4 0.0 copy-start.1
  3.4 2.2 %copy-done.1 = bf16[2048,1024]{1,0:T(8,128)(2,1)S(1)} copy-done((bf16[2048,1024]{1,0:T(8,128)(2,1)S(1)}, bf16[2048,1024]{1,0:T(8,128)(2,1)}, u32[]{:S(2)}) %copy-start.1) | copy-done | bytes 4194328
  5.6 0.0 copy-start.2
  5.6 1.0 copy-done.2
  6.7 0.0 copy-start.3
  6.7 1.0 copy-done.3
  7.7 0.0 copy-start.4
  7.7 1.0 copy-done.4
  8.8 0.0 copy-start.5
  8.8 0.7 copy-done.5
  9.5 2.9 %project.1 = (bf16[1024,128]{1,0:T(8,128)(2,1)S(1)}, bf16[2,128,128]{2,1,0:T(8,128)(2,1)S(1)}) custom-call(bf16[128,2048]{1,0:T(8,128)(2,1)S(1)} %copy-done.2, f32[1,2048]{1,0:T(1,128)S(1)} %bitcast.5, bf16[2048,128]{1,0:T(8,128)(2,1)S(1)} %copy-done.3, bf16[2048,128]{1,0:T(8,128)(2,1)S(1)} %copy-done.4, bf16[2048,1024]{1,0:T(8,128)(2,1)S(1)} %copy-done.1, ...), custom_call_target="tpu_custom_call" | custom-call | flops 671088640 | bytes 6291456 | tf_op jit(solution)/shard_map/project/pallas_call | solution.py:56
  12.4 0.0 copy-done.6
  12.4 34.7 %gather.1 = (bf16[512,128]{1,0:T(8,128)(2,1)S(1)}, bf16[16,8,160,128]{3,2,1,0:T(8,128)(2,1)S(1)}) custom-call(bf16[1024,128]{1,0:T(8,128)(2,1)S(1)} %get-tuple-element.29.q_ref, bf16[2,128,128]{2,1,0:T(8,128)(2,1)S(1)} %get-tuple-element.30.kv_ref, f32[2,1024]{1,0:T(2,128)S(1)} %bitcast.6), custom_call_target="tpu_custom_call" | custom-call | tf_op jit(solution)/shard_map/gather/pallas_call | solution.py:221
  47.1 53.9 %conditional.1 = ((bf16[512,128]{1,0:T(8,128)(2,1)S(1)}, bf16[512,128]{1,0:T(8,128)(2,1)S(1)})) conditional(s32[]{:T(128)} %convert_element_type.3, (bf16[1024,128]{1,0:T(8,128)(2,1)S(1)}, bf16[512,128]{1,0:T(8,128)(2,1)S(1)}, bf16[128,160,128]{2,1,0:T(8,128)(2,1)S(1)}) %tuple.16, (bf16[1024,128]{1,0:T(8,128)(2,1)S(1)}, ...), branch_computations={%region_1.0_spmd, %region_2.0_spmd} | conditional | flops 4563402752 | bytes 6291464 | solution.py:412
  47.1 53.9 %attend_any.1 = (bf16[512,128]{1,0:T(8,128)(2,1)S(1)}, bf16[512,128]{1,0:T(8,128)(2,1)S(1)}) custom-call(bf16[1024,128]{1,0:T(8,128)(2,1)S(1)} %get-tuple-element.17.q_ref, bf16[512,128]{1,0:T(8,128)(2,1)S(1)} %get-tuple-element.18.part_ref, bf16[128,160,128]{2,1,0:T(8,128)(2,1)S(1)} %get-tuple-element.19.kvd_ref), custom_call_target="tpu_custom_call" | custom-call | flops 4563402752 | bytes 6291456 | tf_op jit(solution)/shard_map/cond/branch_0_fun/attend_any/pallas_call | solution.py:335
  101.0 0.0 copy-start
  101.0 2.2 %copy-done = bf16[1024,2048]{1,0:T(8,128)(2,1)S(1)} copy-done((bf16[1024,2048]{1,0:T(8,128)(2,1)S(1)}, bf16[1024,2048]{1,0:T(8,128)(2,1)}, u32[]{:S(2)}) %copy-start) | copy-done | bytes 4194328
  103.2 11.4 %output.1 = bf16[128,2048]{1,0:T(8,128)(2,1)S(1)} custom-call(bf16[512,128]{1,0:T(8,128)(2,1)S(1)} %get-tuple-element.33.oo_ref, bf16[512,128]{1,0:T(8,128)(2,1)S(1)} %get-tuple-element.34.op_ref, bf16[1024,2048]{1,0:T(8,128)(2,1)S(1)} %copy-done), custom_call_target="tpu_custom_call" | custom-call | tf_op jit(solution)/shard_map/output/pallas_call | solution.py:382
  114.6 0.8 copy.17
Async XLA Ops:
  0.0 12.4 %copy-start.6 = (f32[1024,2]{0,1:T(2,128)S(1)}, f32[1024,2]{0,1:T(2,128)}, u32[]{:S(2)}) copy-start(f32[1024,2]{0,1:T(2,128)} %param.18) | copy-start | bytes 24580
  3.4 2.2 %copy-start.1 = (bf16[2048,1024]{1,0:T(8,128)(2,1)S(1)}, bf16[2048,1024]{1,0:T(8,128)(2,1)}, u32[]{:S(2)}) copy-start(bf16[2048,1024]{1,0:T(8,128)(2,1)} %wq_ref.1) | copy-start | bytes 12582916
  5.6 1.0 copy-start.2
  6.7 1.0 copy-start.3
  7.7 1.0 copy-start.4
  8.8 0.7 copy-start.5
  101.0 2.2 %copy-start = (bf16[1024,2048]{1,0:T(8,128)(2,1)S(1)}, bf16[1024,2048]{1,0:T(8,128)(2,1)}, u32[]{:S(2)}) copy-start(bf16[1024,2048]{1,0:T(8,128)(2,1)} %w_ref.1) | copy-start | bytes 12582916

commit v2 on v0

v2 whole, which is shorter than its diff:
```python
import functools

import jax
import jax.numpy as jnp
from jax import lax
from jax.experimental import pallas as pl
from jax.experimental.pallas import tpu as pltpu
from jax.sharding import Mesh
from jax.sharding import PartitionSpec as P

f32 = jnp.float32
bf = jnp.bfloat16
LOG2E = 1.4426950408889634
EPS = 1e-06
MESH = pl.DeviceIdType.MESH
VM = pl.BlockSpec(memory_space=pltpu.VMEM)


def split3(x):
    high = x.astype(bf).astype(f32)
    rest = x - high
    mid = rest.astype(bf).astype(f32)
    return high, mid, rest - mid


def head_norm(flat, heads, gain):
    x = flat.reshape(heads, 64, flat.shape[1])
    scale = lax.rsqrt(jnp.mean(x * x, axis=1, keepdims=True) + EPS)
    return (x * scale * gain[None]).reshape(flat.shape)


HBM = pl.BlockSpec(memory_space=pltpu.HBM)
SEQ_J = (0, 3, 1, 0, 0, 2, 0, 3, 3, 1, 1, 3, 1, 2, 2, 2)
SEQ_K = (0, 0, 0, 3, 1, 0, 2, 3, 1, 3, 1, 2, 2, 3, 1, 2)


def column(row):
    return jnp.broadcast_to(row, (128, 64)).T


def start_kernel(x_hbm, gain_ref, wk_hbm, wv_hbm, qg_ref, kg_ref, norm_ref, kv_ref, bound_ref, *scratch):
    x_ref, wk_ref, wv_ref, sems = scratch
    copies = [
        pltpu.make_async_copy(src, dst, sems.at[i])
        for i, (src, dst) in enumerate(((x_hbm, x_ref), (wk_hbm, wk_ref), (wv_hbm, wv_ref)))
    ]
    for copy in copies:
        copy.start()
    bound_ref[0] = 8.0 * 1.02 * jnp.max(jnp.abs(qg_ref[...] * kg_ref[...]))
    gain = column(kg_ref[...])
    copies[0].wait()
    x = x_ref[...].astype(f32)
    scale = lax.rsqrt(jnp.mean(x * x, axis=1, keepdims=True) + EPS)
    norm_ref[...] = (x * scale * gain_ref[...]).astype(bf)
    copies[1].wait()
    keys = jnp.dot(norm_ref[...], wk_ref[...], preferred_element_type=f32)
    copies[2].wait()
    values = jnp.dot(norm_ref[...], wv_ref[...], preferred_element_type=f32)
    keys = head_norm(keys.T, 2, gain).astype(bf)
    values = values.T.astype(bf)
    for g in range(2):
        kv_ref[g, 0:64] = keys[g * 64 : (g + 1) * 64]
        kv_ref[g, 64:128] = values[g * 64 : (g + 1) * 64]


def start(x, gain, wk, wv, qg, kg):
    return pl.pallas_call(
        start_kernel,
        out_shape=[
            jax.ShapeDtypeStruct((128, 2048), bf),
            jax.ShapeDtypeStruct((2, 128, 128), bf),
            jax.ShapeDtypeStruct((1,), f32),
        ],
        in_specs=[HBM, VM, HBM, HBM, VM, VM],
        out_specs=[VM, VM, pl.BlockSpec(memory_space=pltpu.SMEM)],
        scratch_shapes=[
            pltpu.VMEM((128, 2048), bf),
            pltpu.VMEM((2048, 128), bf),
            pltpu.VMEM((2048, 128), bf),
            pltpu.SemaphoreType.DMA((3,)),
        ],
        compiler_params=pltpu.CompilerParams(vmem_limit_bytes=60 * 1024 * 1024),
        cost_estimate=pl.CostEstimate(
            flops=2 * 128 * 2048 * 256, bytes_accessed=2 * 1024 * 1024, transcendentals=0
        ),
        name="start",
    )(x, gain, wk, wv, qg, kg)


def load_keys(all_ref, line, p, ref_d, ones):
    dec = all_ref[line, p, 128:152].astype(f32)
    rel = dec[0:8] + dec[8:16] + dec[16:24] - ref_d
    rows = jnp.concatenate([*split3(rel), ones], axis=0).astype(bf)
    full = jnp.concatenate([all_ref[line, p, 0:64], rows, jnp.zeros((32, 128), bf)], axis=0)
    return full.T, all_ref[line, p, 64:128]


def main_kernel(bounded, tile, norm_ref, kv_ref, d_ref, qg_ref, wq_hbm, wo_hbm, out_ref, *scratch):
    all_ref, dec_ref, far_ref, wq_ref, wo_ref, part_ref = scratch[:6]
    qs_ref, qr_ref, os_ref, near_ref, got_ref = scratch[6:11]
    qa_ref, acc_ref, sum_ref, max_ref, refd_ref = scratch[11:16]
    w_sem, p_send, p_recv, d_send, d_recv, x_send, x_recv, r_send, r_recv, s_send, s_recv = scratch[16:]
    z, y, x, c = (lax.axis_index(n) for n in ("z", "y", "x", "c"))
    g = x // 2
    tp = 2 * x + c
    own_line = 4 * z + y
    mine = (x - 2 * g) * 2 + c
    mirror = (3 - z, 3 - y, 3 - x, 1 - c)
    across = (3 - z, 3 - y, x, c)
    sibling = (z, y, x, 1 - c)
    a = (1 - c) * y + c * z
    b = (1 - c) * z + c * y

    def line_at(j, k):
        pa, pb = lax.rem(a + j, 4), lax.rem(b + k, 4)
        return (1 - c) * (4 * pb + pa) + c * (4 * pa + pb)

    def at_ab(j, k):
        pa, pb = lax.rem(a + j, 4), lax.rem(b + k, 4)
        return ((1 - c) * pb + c * pa, (1 - c) * pa + c * pb, x, c)

    up_a, down_a, up_b, down_b = at_ab(1, 0), at_ab(3, 0), at_ab(0, 1), at_ab(0, 3)

    def remote(src, dst, send_sem, recv_sem, peer):
        return pltpu.make_async_remote_copy(
            src_ref=src,
            dst_ref=dst,
            send_sem=send_sem,
            recv_sem=recv_sem,
            device_id=peer,
            device_id_type=MESH,
        )

    w_far = pl.multiple_of((1 - g) * 512, 512)
    w_near = pl.multiple_of(g * 512, 512)
    far_copy = pltpu.make_async_copy(wq_hbm.at[:, pl.ds(w_far, 512)], wq_ref.at[0], w_sem.at[0])
    near_copy = pltpu.make_async_copy(wq_hbm.at[:, pl.ds(w_near, 512)], wq_ref.at[1], w_sem.at[1])
    out_copy = pltpu.make_async_copy(wo_hbm, wo_ref, w_sem.at[2])

    barrier = pltpu.get_barrier_semaphore()
    peers = [(z, y, lax.rem(x + k, 4), cc) for k in range(1, 4) for cc in range(2)]
    peers += [sibling, mirror, across, up_a, down_a, up_b, down_b]
    for peer in peers:
        pl.semaphore_signal(barrier, inc=1, device_id=peer, device_id_type=MESH)
    far_copy.start()
    near_copy.start()
    dec_ref[mine] = d_ref[...]

    @pl.when(g == c)
    def _():
        all_ref[own_line, tp, 0:128] = kv_ref[g]

    gain = column(qg_ref[...])
    pl.semaphore_wait(barrier, len(peers))

    def decay_copy(k):
        t = lax.rem(mine + k, 4)
        peer = (z, y, 2 * g + t // 2, lax.rem(t, 2))
        return remote(d_ref, dec_ref.at[mine], d_send.at[k], d_recv.at[k], peer)

    def piece_copy(k):
        to = lax.rem(x + k, 4)
        slot = (x - 2 * g) * 2 + c
        return remote(
            kv_ref.at[to // 2],
            all_ref.at[own_line, tp, pl.ds(0, 128)],
            p_send.at[k],
            p_recv.at[slot],
            (z, y, to, g),
        )

    for k in range(1, 4):
        decay_copy(k).start()
    for k in range(1, 4):
        piece_copy(k).start()

    @pl.when(g != c)
    def _():
        piece_copy(0).start()

    def queries(slot):
        flat = jnp.dot(norm_ref[...], wq_ref[slot], preferred_element_type=f32)
        return (head_norm(flat.T, 8, gain) * (LOG2E / 8)).astype(bf)

    far_copy.wait()
    qs_ref[...] = queries(0)

    for k in range(1, 4):
        decay_copy(k).wait_recv()
    for i in range(4):
        first = pl.multiple_of((4 * c + i) * 128, 128)
        value = jnp.concatenate([dec_ref[q, :, pl.ds(first, 128)] for q in range(4)], axis=0)
        all_ref[own_line, 4 * c + i, 128:152] = jnp.concatenate(
            split3(value * LOG2E), axis=0
        ).astype(bf)
    far_first = pl.multiple_of((7 - tp) * 128, 128)
    far_decays = remote(
        dec_ref.at[:, :, pl.ds(far_first, 128)], far_ref, x_send.at[0], x_recv.at[0], across
    )
    far_decays.start()
    q_copy = remote(qs_ref, qr_ref, x_send.at[1], x_recv.at[1], mirror)
    q_copy.start()

    def block(line, sub):
        return all_ref.at[line, pl.ds(4 * c + 2 * sub, 2)]

    def ring(step, slot):
        side = (0, 0, 0, 0, 3, 1)[slot]
        sub = (0, 1, 0, 1, 0, 1)[slot]
        upward = slot in (0, 1, 4)
        if step == 0:
            line, peer = line_at(side, 0), (up_a if upward else down_a)
        else:
            line, peer = line_at(step - 1, side), (up_b if upward else down_b)
        index = step * 6 + slot
        ref = block(line, sub)
        return remote(ref, ref, r_send.at[index], r_recv.at[index], peer)

    def share(j, k):
        half = all_ref.at[line_at(j, k), pl.ds(4 * c, 4)]
        index = j * 4 + k
        return remote(half, half, s_send.at[index], s_recv.at[index], sibling)

    def ring_start(step):
        for slot in range(4):
            ring(step, slot).start()

    def ring_relay(step):
        ring(step, 0).wait_recv()
        ring(step, 4).start()
        ring(step, 3).wait_recv()
        ring(step, 5).start()
        ring(step, 1).wait_recv()
        ring(step, 2).wait_recv()

    def ring_end(step):
        ring(step, 4).wait_recv()
        ring(step, 5).wait_recv()

    for i in range(4):

        @pl.when(4 * c + i != tp)
        def _():
            remote(
                kv_ref.at[0],
                all_ref.at[own_line, 4 * c + i, pl.ds(0, 128)],
                p_send.at[0],
                p_recv.at[i],
                sibling,
            ).wait_recv()

    ring_start(0)
    ring_start(1)
    share(0, 0).start()

    row8 = lax.broadcasted_iota(jnp.int32, (8, 128), 0)
    ones = jnp.where(row8 < 3, 1.0, 0.0).astype(f32)

    def prepare(rg, query_ref, decays):
        ref_d = jnp.broadcast_to(decays[:, 0:1], (8, 128))
        refd_ref[rg] = ref_d
        parts = split3(decays - ref_d)
        for h in range(8):
            onehot = jnp.where(row8 == h, -1.0, 0.0).astype(f32)
            own = jnp.zeros((8, 128), f32)
            for i, part in enumerate(parts):
                own = jnp.where(row8 == i, part[h : h + 1], own)
            rows = jnp.concatenate([onehot, onehot, onehot, own], axis=0).astype(bf)
            qa_ref[rg, :, h * 128 : (h + 1) * 128] = jnp.concatenate(
                [query_ref[h * 64 : (h + 1) * 64, :], rows, jnp.zeros((32, 128), bf)], axis=0
            )

    near_copy.wait()
    out_copy.start()
    near_ref[...] = queries(1)
    here = pl.multiple_of(tp * 128, 128)
    own_decays = jnp.concatenate([dec_ref[q, :, pl.ds(here, 128)] for q in range(4)], axis=0)
    prepare(0, near_ref, own_decays * LOG2E)
    acc_ref[...] = jnp.zeros_like(acc_ref)
    sum_ref[...] = jnp.zeros_like(sum_ref)
    if not bounded:
        max_ref[...] = jnp.full(max_ref.shape, -1e30, f32)

    def attend(rg, line, tp_row, masked):
        ref_d = refd_ref[rg]
        loaded = [load_keys(all_ref, line, p, ref_d, ones) for p in range(8)]
        keys = jnp.concatenate([k for k, _ in loaded], axis=0)
        values = jnp.concatenate([v for _, v in loaded], axis=1)
        for n in range(1024 // tile):
            cols = slice(n * tile, (n + 1) * tile)
            scores = jnp.dot(keys, qa_ref[rg, :, cols], preferred_element_type=f32)
            if masked:
                key_pos = lax.broadcasted_iota(jnp.int32, (1024, tile), 0)
                query_pos = tp_row * 128 + (lax.broadcasted_iota(jnp.int32, (1024, tile), 1) & 127)
                scores = jnp.where(key_pos <= query_pos, scores, -1e30)
            if bounded:
                weights = jnp.exp2(scores)
                sum_ref[rg, :, cols] += jnp.sum(weights.reshape(128, 8, tile), axis=0)
                acc_ref[rg, :, cols] += jnp.dot(
                    values, weights.astype(bf), preferred_element_type=f32
                )
            else:
                old = max_ref[rg, 0:1, cols]
                new = jnp.maximum(old, jnp.max(scores, axis=0, keepdims=True))
                keep = jnp.exp2(old - new)
                weights = jnp.exp2(scores - new)
                max_ref[rg, :, cols] = jnp.broadcast_to(new, (8, tile))
                sums = jnp.sum(weights.reshape(128, 8, tile), axis=0)
                sum_ref[rg, :, cols] = sum_ref[rg, :, cols] * keep + sums
                acc_ref[rg, :, cols] = acc_ref[rg, :, cols] * keep + jnp.dot(
                    values, weights.astype(bf), preferred_element_type=f32
                )

    def act_1():
        ring_relay(0)
        share(3, 0).start()
        share(1, 0).start()
        ring_relay(1)
        ring_start(4)
        ring_start(2)
        share(0, 3).start()
        share(0, 1).start()

    def act_3():
        ring_end(0)
        ring_start(3)
        share(2, 0).start()
        ring_end(1)
        share(0, 2).start()

    def act_6():
        for j in (3, 1):
            ring_relay(1 + j)
            share(j, 3).start()
            share(j, 1).start()

    def act_9():
        ring_relay(3)
        share(2, 3).start()
        share(2, 1).start()
        for j in (3, 1):
            ring_end(1 + j)
            share(j, 2).start()

    def act_13():
        ring_end(3)
        share(2, 2).start()

    actions = {1: act_1, 3: act_3, 6: act_6, 9: act_9, 13: act_13}

    def table(values, step):
        total = 0
        for i, value in enumerate(values):
            if value:
                total = total + value * (step == i).astype(jnp.int32)
        return total

    def body(step, carry):
        for at, action in actions.items():

            @pl.when(step == at)
            def _(action=action):
                action()

        j, k = table(SEQ_J, step), table(SEQ_K, step)
        line = line_at(j, k)
        index = k * 4 + j
        half = all_ref.at[line, pl.ds(4 * (1 - c), 4)]
        remote(half, half, s_send.at[index], s_recv.at[index], sibling).wait_recv()

        def group(rg, inner):
            @pl.when((step == 0) & (rg == 1))
            def _():
                far_decays.wait_recv()
                q_copy.wait_recv()
                far = jnp.concatenate([far_ref[q] for q in range(4)], axis=0)
                prepare(1, qr_ref, far * LOG2E)

            last = own_line + rg * (15 - 2 * own_line)
            tp_row = tp + rg * (7 - 2 * tp)

            @pl.when(line < last)
            def _():
                attend(rg, line, tp_row, False)

            @pl.when(line == last)
            def _():
                attend(rg, line, tp_row, True)

            return inner

        return lax.fori_loop(0, 2, group, carry)

    lax.fori_loop(0, 16, body, 0)

    def finish(rg, to_ref):
        inverse = 1.0 / jnp.sum(sum_ref[rg], axis=0, keepdims=True)
        for h in range(8):
            cols = slice(h * 128, (h + 1) * 128)
            to_ref[h * 64 : (h + 1) * 64, :] = (acc_ref[rg, :, cols] * inverse[:, cols]).astype(bf)

    finish(1, os_ref)
    finish(0, near_ref)
    back = remote(os_ref, got_ref, x_send.at[2], x_recv.at[2], mirror)
    back.start()
    out_copy.wait()
    near = near_ref[...].T
    for n in range(4):
        cols = slice(n * 512, (n + 1) * 512)
        part_ref[:, cols] = jnp.dot(near, wo_ref[pl.ds(w_near, 512), cols], preferred_element_type=f32)
    for k in range(1, 4):
        decay_copy(k).wait_send()
        piece_copy(k).wait_send()

    @pl.when(g != c)
    def _():
        piece_copy(0).wait_send()

    far_decays.wait_send()
    q_copy.wait_send()
    for step in range(5):
        for slot in range(6):
            ring(step, slot).wait_send()
    for j in range(4):
        for k in range(4):
            share(j, k).wait_send()
    back.wait_recv()
    far = got_ref[...].T
    for n in range(4):
        cols = slice(n * 512, (n + 1) * 512)
        rest = jnp.dot(far, wo_ref[pl.ds(w_far, 512), cols], preferred_element_type=f32)
        out_ref[:, cols] = (part_ref[:, cols] + rest).astype(bf)
    back.wait_send()


def main(norm, kv, d, qg, wq, wo, bounded):
    dma = lambda *n: pltpu.SemaphoreType.DMA(n)
    return pl.pallas_call(
        functools.partial(main_kernel, bounded, 512 if bounded else 256),
        out_shape=jax.ShapeDtypeStruct((128, 2048), bf),
        in_specs=[VM, VM, VM, VM, HBM, HBM],
        out_specs=VM,
        scratch_shapes=[
            pltpu.VMEM((16, 8, 152, 128), bf),
            pltpu.VMEM((4, 2, 1024), f32),
            pltpu.VMEM((4, 2, 128), f32),
            pltpu.VMEM((2, 2048, 512), bf),
            pltpu.VMEM((1024, 2048), bf),
            pltpu.VMEM((128, 2048), f32),
            pltpu.VMEM((512, 128), bf),
            pltpu.VMEM((512, 128), bf),
            pltpu.VMEM((512, 128), bf),
            pltpu.VMEM((512, 128), bf),
            pltpu.VMEM((512, 128), bf),
            pltpu.VMEM((2, 128, 1024), bf),
            pltpu.VMEM((2, 64, 1024), f32),
            pltpu.VMEM((2, 8, 1024), f32),
            pltpu.VMEM((2, 8, 1024), f32),
            pltpu.VMEM((2, 8, 128), f32),
            dma(3),
            dma(4),
            dma(4),
            dma(4),
            dma(4),
            dma(3),
            dma(3),
            dma(30),
            dma(30),
            dma(16),
            dma(16),
        ],
        compiler_params=pltpu.CompilerParams(
            collective_id=0 if bounded else 1,
            has_side_effects=True,
            vmem_limit_bytes=60 * 1024 * 1024,
        ),
        name="main_bounded" if bounded else "main_any",
    )(norm, kv, d, qg, wq, wo)


def per_device(inputs, in_gain, w_query, w_key, w_value, query_gain, key_gain, decay_sums, w_out):
    query_gain = query_gain.reshape(1, -1)
    key_gain = key_gain.reshape(1, -1)
    norm, kv, bound = start(inputs, in_gain.reshape(1, -1), w_key, w_value, query_gain, key_gain)
    return lax.cond(
        bound[0] <= 64.0,
        lambda *a: main(*a, True),
        lambda *a: main(*a, False),
        norm,
        kv,
        decay_sums.T,
        query_gain,
        w_query,
        w_out,
    )


def solution(mesh):
    torus = Mesh(mesh.devices.reshape(4, 4, 4, 2), ("z", "y", "x", "c"))
    every = ("z", "y", "x", "c")
    in_specs = (P(every, None), P(), P(), P(), P(), P(), P(), P(("z", "y"), ("x", "c")), P())
    return jax.shard_map(
        per_device, mesh=torus, in_specs=in_specs, out_specs=P(every, None), check_vma=False
    )
```

time: 269 us -> 87.2 us (0.32); the launches traced: 265 us -> 87 us
  Pallas kernels: 0 us -> 85.5 us
  local copies, waits for them, and re-layouts: 63.6 us -> 0.8 us
  waiting for transfers between devices: 52.6 us -> 0 us
  matrix products: 43.4 us -> 0 us
  blocking collectives: 32 us -> 0 us
  loops' own time: 27.2 us -> 0.02 us
  starting transfers between devices: 18.8 us -> 0 us
  other arithmetic: 13.4 us -> 0 us
  between operations: 13.7 us -> 0.67 us
    pallas_call x0 -> x2, Pallas kernels: none -> 85.5 us  [the longest x1 82.7 us: main(): pl.pallas_call(functools.partial(main_kernel, bounded, 512 if bounded els...]
    dot_general x70 -> x0, matrix products: 43.4 us -> none  [the longest x33 17.1 us: attend_step(): jnp.einsum('htu,ud->thd', weights_exp.astype(jnp.bfloat16), value_slice,...]
    slice x36 -> x0, local copies, waits for them, and re-layouts: 36.1 us -> none  [the longest x32 35.1 us: one_block(): value_slice = pair_slice[:, head_size:]]
    all_to_all x3 -> x0, blocking collectives: 32 us -> none  [the longest x2 17.9 us: moved_by_axis(): filled = lax.all_to_all(filled, axes[k], k, k, tiled=True)]
    all_gather x1 -> x0, waiting for transfers between devices: 28.2 us -> none  [per_device(): pieces = lax.all_gather(key_values, 'sp', axis=0, tiled=True)]
    another operation x65 -> x1, loops' own time: 27.2 us -> 0.02 us  [per_device(): lax.cond(bound[0] <= 64.0, lambda *a: main(*a, True), lambda *a: main(*a,...]
    ppermute x8 -> x0, waiting for transfers between devices: 20.7 us -> none  [partner(): lax.ppermute(value, axis, [(i, i ^ 1 << stride) for i in range(lax.axis_s...]
    dynamic_slice x32 -> x0, local copies, waits for them, and re-layouts: 18.8 us -> none  [per_device(): lax.scan(one_block, state, jnp.arange(piece_rows // key_block, dtype=jnp....]
  transfers between devices with their start and end apart: 10 -> 0, of which waited for: 9 -> 0; matrix products, arithmetic and copies ran while one was open for 0% -> 0% of each run, Pallas kernels for 0% -> 0%
where the time goes in v2:
time: 87.2 us; the launch traced here: 87 us
  Pallas kernels  85.5 us (98%)
    pallas_call x1, Pallas kernels, main(): pl.pallas_call(functools.partial(main_kernel, bounded, 512 if bounded els...  82.7 us
    pallas_call x1, Pallas kernels, start(): pl.pallas_call(start_kernel, out_shape=[jax.ShapeDtypeStruct((128, 2048),...  2.81 us

profile of v2, /device:TPU:33, one launch (start us, length us, event | category | flops | bytes accessed | tf_op | source)
XLA Modules:
  0.0 87.0 jit_solution(12596934999188688748)
XLA Ops:
  0.0 2.8 %start.1 = (bf16[128,2048]{1,0:T(8,128)(2,1)S(1)}, bf16[2,128,128]{2,1,0:T(8,128)(2,1)S(1)}, f32[1]{0:T(128)}) custom-call(bf16[128,2048]{1,0:T(8,128)(2,1)} %x_hbm.1, f32[1,2048]{1,0:T(1,128)} %bitcast.7, bf16[2048,128]{1,0:T(8,128)(2,1)} %wk_hbm.1, bf16[2048,128]{1,0:T(8,128)(2,1)} %wv_hbm.1, f32[1,64]{1,0:T(1,128)} %bitcast.8, f32[1,64]{1,0:T(1,128)} %bitcast.11), custom_call_target="tpu_custom_call" | custom-call | flops 134217728 | bytes 2097152 | tf_op jit(solution)/shard_map/start/pallas_call | solution.py:67
  3.5 82.7 %conditional.1 = (bf16[128,2048]{1,0:T(8,128)(2,1)S(1)}) conditional(s32[]{:T(128)} %bitcast.3, (bf16[128,2048]{1,0:T(8,128)(2,1)S(1)}, bf16[2,128,128]{2,1,0:T(8,128)(2,1)S(1)}, f32[2,1024]{1,0:T(2,128)}, f32[1,64]{1,0:T(1,128)}, bf16[2048,1024]{1,0:T(8,128)(2,1)}, /*index=5*/bf16[1024,2048]{1,0:T(8,128)(2,1)}) %tuple.18, ...), branch_computations={%region_0.0_spmd, %region_1.0_spmd} | conditional | bytes 8 | solution.py:485
  3.5 82.7 %main_any.1 = bf16[128,2048]{1,0:T(8,128)(2,1)S(1)} custom-call(bf16[128,2048]{1,0:T(8,128)(2,1)S(1)} %get-tuple-element.32.norm_ref, bf16[2,128,128]{2,1,0:T(8,128)(2,1)S(1)} %get-tuple-element.33.kv_ref, f32[2,1024]{1,0:T(2,128)} %get-tuple-element.34.d_ref, f32[1,64]{1,0:T(1,128)} %get-tuple-element.35.qg_ref, ...), custom_call_target="tpu_custom_call" | custom-call | tf_op jit(solution)/shard_map/cond/branch_0_fun/main_any/pallas_call | solution.py:438
  86.2 0.8 copy.19

commit v3 on v2

--- a/solution.py
+++ b/solution.py
@@ -32,59 +32,20 @@
 HBM = pl.BlockSpec(memory_space=pltpu.HBM)
 SEQ_J = (0, 3, 1, 0, 0, 2, 0, 3, 3, 1, 1, 3, 1, 2, 2, 2)
 SEQ_K = (0, 0, 0, 3, 1, 0, 2, 3, 1, 3, 1, 2, 2, 3, 1, 2)
+ROWS, LAG = 256, 3
+
+
+def packed(values):
+    total = sum(v << 2 * i for i, v in enumerate(values))
+    return total - (1 << 32) if total >> 31 else total
+
+
+def unpacked(values, index):
+    return lax.shift_right_logical(jnp.int32(packed(values)), 2 * index) & 3
 
 
 def column(row):
     return jnp.broadcast_to(row, (128, 64)).T
-
-
-def start_kernel(x_hbm, gain_ref, wk_hbm, wv_hbm, qg_ref, kg_ref, norm_ref, kv_ref, bound_ref, *scratch):
-    x_ref, wk_ref, wv_ref, sems = scratch
-    copies = [
-        pltpu.make_async_copy(src, dst, sems.at[i])
-        for i, (src, dst) in enumerate(((x_hbm, x_ref), (wk_hbm, wk_ref), (wv_hbm, wv_ref)))
-    ]
-    for copy in copies:
-        copy.start()
-    bound_ref[0] = 8.0 * 1.02 * jnp.max(jnp.abs(qg_ref[...] * kg_ref[...]))
-    gain = column(kg_ref[...])
-    copies[0].wait()
-    x = x_ref[...].astype(f32)
-    scale = lax.rsqrt(jnp.mean(x * x, axis=1, keepdims=True) + EPS)
-    norm_ref[...] = (x * scale * gain_ref[...]).astype(bf)
-    copies[1].wait()
-    keys = jnp.dot(norm_ref[...], wk_ref[...], preferred_element_type=f32)
-    copies[2].wait()
-    values = jnp.dot(norm_ref[...], wv_ref[...], preferred_element_type=f32)
-    keys = head_norm(keys.T, 2, gain).astype(bf)
-    values = values.T.astype(bf)
-    for g in range(2):
-        kv_ref[g, 0:64] = keys[g * 64 : (g + 1) * 64]
-        kv_ref[g, 64:128] = values[g * 64 : (g + 1) * 64]
-
-
-def start(x, gain, wk, wv, qg, kg):
-    return pl.pallas_call(
-        start_kernel,
-        out_shape=[
-            jax.ShapeDtypeStruct((128, 2048), bf),
-            jax.ShapeDtypeStruct((2, 128, 128), bf),
-            jax.ShapeDtypeStruct((1,), f32),
-        ],
-        in_specs=[HBM, VM, HBM, HBM, VM, VM],
-        out_specs=[VM, VM, pl.BlockSpec(memory_space=pltpu.SMEM)],
-        scratch_shapes=[
-            pltpu.VMEM((128, 2048), bf),
-            pltpu.VMEM((2048, 128), bf),
-            pltpu.VMEM((2048, 128), bf),
-            pltpu.SemaphoreType.DMA((3,)),
-        ],
-        compiler_params=pltpu.CompilerParams(vmem_limit_bytes=60 * 1024 * 1024),
-        cost_estimate=pl.CostEstimate(
-            flops=2 * 128 * 2048 * 256, bytes_accessed=2 * 1024 * 1024, transcendentals=0
-        ),
-        name="start",
-    )(x, gain, wk, wv, qg, kg)
 
 
 def load_keys(all_ref, line, p, ref_d, ones):
@@ -92,14 +53,18 @@
     rel = dec[0:8] + dec[8:16] + dec[16:24] - ref_d
     rows = jnp.concatenate([*split3(rel), ones], axis=0).astype(bf)
     full = jnp.concatenate([all_ref[line, p, 0:64], rows, jnp.zeros((32, 128), bf)], axis=0)
-    return full.T, all_ref[line, p, 64:128]
-
-
-def main_kernel(bounded, tile, norm_ref, kv_ref, d_ref, qg_ref, wq_hbm, wo_hbm, out_ref, *scratch):
+    return full.T
+
+
+def main_kernel(bounded, tile, *refs):
+    x_hbm, in_gain_ref, wk_hbm, wv_hbm, qg_ref, kg_ref, d_ref, wq_hbm, wo_hbm = refs[:9]
+    out_ref, bound_ref = refs[9:11]
+    x_ref, wk_ref, wv_ref, norm_ref, kv_ref = refs[11:16]
+    scratch = refs[16:]
     all_ref, dec_ref, far_ref, wq_ref, wo_ref, part_ref = scratch[:6]
     qs_ref, qr_ref, os_ref, near_ref, got_ref = scratch[6:11]
-    qa_ref, acc_ref, sum_ref, max_ref, refd_ref = scratch[11:16]
-    w_sem, p_send, p_recv, d_send, d_recv, x_send, x_recv, r_send, r_recv, s_send, s_recv = scratch[16:]
+    qa_ref, acc_ref, sum_ref, max_ref, refd_ref, ka_ref, wt_ref = scratch[11:18]
+    w_sem, p_send, p_recv, d_send, d_recv, x_send, x_recv, r_send, r_recv, s_send, s_recv = scratch[18:]
     z, y, x, c = (lax.axis_index(n) for n in ("z", "y", "x", "c"))
     g = x // 2
     tp = 2 * x + c
@@ -112,11 +77,11 @@
     b = (1 - c) * z + c * y
 
     def line_at(j, k):
-        pa, pb = lax.rem(a + j, 4), lax.rem(b + k, 4)
+        pa, pb = (a + j) & 3, (b + k) & 3
         return (1 - c) * (4 * pb + pa) + c * (4 * pa + pb)
 
     def at_ab(j, k):
-        pa, pb = lax.rem(a + j, 4), lax.rem(b + k, 4)
+        pa, pb = (a + j) & 3, (b + k) & 3
         return ((1 - c) * pb + c * pa, (1 - c) * pa + c * pb, x, c)
 
     up_a, down_a, up_b, down_b = at_ab(1, 0), at_ab(3, 0), at_ab(0, 1), at_ab(0, 3)
@@ -137,6 +102,12 @@
     near_copy = pltpu.make_async_copy(wq_hbm.at[:, pl.ds(w_near, 512)], wq_ref.at[1], w_sem.at[1])
     out_copy = pltpu.make_async_copy(wo_hbm, wo_ref, w_sem.at[2])
 
+    first_copies = [
+        pltpu.make_async_copy(src, dst, w_sem.at[3 + i])
+        for i, (src, dst) in enumerate(((x_hbm, x_ref), (wk_hbm, wk_ref), (wv_hbm, wv_ref)))
+    ]
+    for copy in first_copies:
+        copy.start()
     barrier = pltpu.get_barrier_semaphore()
     peers = [(z, y, lax.rem(x + k, 4), cc) for k in range(1, 4) for cc in range(2)]
     peers += [sibling, mirror, across, up_a, down_a, up_b, down_b]
@@ -145,12 +116,28 @@
     far_copy.start()
     near_copy.start()
     dec_ref[mine] = d_ref[...]
+    bound_ref[0] = 8.0 * 1.02 * jnp.max(jnp.abs(qg_ref[...] * kg_ref[...]))
+    gain = column(qg_ref[...])
+    key_gain = column(kg_ref[...])
+
+    first_copies[0].wait()
+    rows = x_ref[...].astype(f32)
+    scale = lax.rsqrt(jnp.mean(rows * rows, axis=1, keepdims=True) + EPS)
+    norm_ref[...] = (rows * scale * in_gain_ref[...]).astype(bf)
+    first_copies[1].wait()
+    keys = jnp.dot(norm_ref[...], wk_ref[...], preferred_element_type=f32)
+    first_copies[2].wait()
+    values = jnp.dot(norm_ref[...], wv_ref[...], preferred_element_type=f32)
+    keys = head_norm(keys.T, 2, key_gain).astype(bf)
+    values = values.T.astype(bf)
+    for i in range(2):
+        kv_ref[i, 0:64] = keys[i * 64 : (i + 1) * 64]
+        kv_ref[i, 64:128] = values[i * 64 : (i + 1) * 64]
 
     @pl.when(g == c)
     def _():
         all_ref[own_line, tp, 0:128] = kv_ref[g]
 
-    gain = column(qg_ref[...])
     pl.semaphore_wait(barrier, len(peers))
 
     def decay_copy(k):
@@ -199,7 +186,11 @@
     )
     far_decays.start()
     q_copy = remote(qs_ref, qr_ref, x_send.at[1], x_recv.at[1], mirror)
-    q_copy.start()
+    late = own_line < 8
+
+    @pl.when(jnp.logical_not(late))
+    def _():
+        q_copy.start()
 
     def block(line, sub):
         return all_ref.at[line, pl.ds(4 * c + 2 * sub, 2)]
@@ -283,39 +274,62 @@
 
     def attend(rg, line, tp_row, masked):
         ref_d = refd_ref[rg]
-        loaded = [load_keys(all_ref, line, p, ref_d, ones) for p in range(8)]
-        keys = jnp.concatenate([k for k, _ in loaded], axis=0)
-        values = jnp.concatenate([v for _, v in loaded], axis=1)
-        for n in range(1024 // tile):
+        for p in range(8):
+            ka_ref[p * 128 : (p + 1) * 128] = load_keys(all_ref, line, p, ref_d, ones)
+        units = [(m, n) for m in range(1024 // ROWS) for n in range(1024 // tile)]
+
+        def weigh(u):
+            m, n = units[u]
             cols = slice(n * tile, (n + 1) * tile)
+            keys = ka_ref[m * ROWS : (m + 1) * ROWS]
             scores = jnp.dot(keys, qa_ref[rg, :, cols], preferred_element_type=f32)
             if masked:
-                key_pos = lax.broadcasted_iota(jnp.int32, (1024, tile), 0)
-                query_pos = tp_row * 128 + (lax.broadcasted_iota(jnp.int32, (1024, tile), 1) & 127)
+                shape = (ROWS, tile)
+                key_pos = m * ROWS + lax.broadcasted_iota(jnp.int32, shape, 0)
+                query_pos = tp_row * 128 + (lax.broadcasted_iota(jnp.int32, shape, 1) & 127)
                 scores = jnp.where(key_pos <= query_pos, scores, -1e30)
             if bounded:
                 weights = jnp.exp2(scores)
-                sum_ref[rg, :, cols] += jnp.sum(weights.reshape(128, 8, tile), axis=0)
-                acc_ref[rg, :, cols] += jnp.dot(
-                    values, weights.astype(bf), preferred_element_type=f32
-                )
+                sum_ref[rg, :, cols] += jnp.sum(weights.reshape(ROWS // 8, 8, tile), axis=0)
             else:
                 old = max_ref[rg, 0:1, cols]
                 new = jnp.maximum(old, jnp.max(scores, axis=0, keepdims=True))
                 keep = jnp.exp2(old - new)
                 weights = jnp.exp2(scores - new)
                 max_ref[rg, :, cols] = jnp.broadcast_to(new, (8, tile))
-                sums = jnp.sum(weights.reshape(128, 8, tile), axis=0)
+                sums = jnp.sum(weights.reshape(ROWS // 8, 8, tile), axis=0)
                 sum_ref[rg, :, cols] = sum_ref[rg, :, cols] * keep + sums
-                acc_ref[rg, :, cols] = acc_ref[rg, :, cols] * keep + jnp.dot(
-                    values, weights.astype(bf), preferred_element_type=f32
-                )
+                acc_ref[rg, :, cols] = acc_ref[rg, :, cols] * keep
+            wt_ref[u % (lag + 1)] = weights.astype(bf)
+
+        def gather_values(u):
+            m, n = units[u]
+            cols = slice(n * tile, (n + 1) * tile)
+            first = m * ROWS // 128
+            values = jnp.concatenate(
+                [all_ref[line, p, 64:128] for p in range(first, first + ROWS // 128)], axis=1
+            )
+            acc_ref[rg, :, cols] += jnp.dot(
+                values, wt_ref[u % (lag + 1)], preferred_element_type=f32
+            )
+
+        lag = LAG if bounded else 0
+        for u in range(len(units) + lag):
+            if u < len(units):
+                weigh(u)
+            if u >= lag:
+                gather_values(u - lag)
 
     def act_1():
         ring_relay(0)
         share(3, 0).start()
         share(1, 0).start()
         ring_relay(1)
+
+        @pl.when(late)
+        def _():
+            q_copy.start()
+
         ring_start(4)
         ring_start(2)
         share(0, 3).start()
@@ -346,14 +360,9 @@
         ring_end(3)
         share(2, 2).start()
 
-    actions = {1: act_1, 3: act_3, 6: act_6, 9: act_9, 13: act_13}
-
-    def table(values, step):
-        total = 0
-        for i, value in enumerate(values):
-            if value:
-                total = total + value * (step == i).astype(jnp.int32)
-        return total
+    actions = {1: act_1, 4: act_3, 7: act_6, 10: act_9, 14: act_13}
+
+    later = jnp.where(late, 0, 1)
 
     def body(step, carry):
         for at, action in actions.items():
@@ -362,20 +371,25 @@
             def _(action=action):
                 action()
 
-        j, k = table(SEQ_J, step), table(SEQ_K, step)
-        line = line_at(j, k)
-        index = k * 4 + j
-        half = all_ref.at[line, pl.ds(4 * (1 - c), 4)]
-        remote(half, half, s_send.at[index], s_recv.at[index], sibling).wait_recv()
+        place = jnp.maximum(step - 1, 0) & 15
+        j, k = unpacked(SEQ_J, place), unpacked(SEQ_K, place)
+        again = (step >= 17).astype(jnp.int32)
+        line = line_at(j, k) * (1 - again) + (step - 17) * again
+
+        @pl.when((step != 1) & (step < 17))
+        def _():
+            index = k * 4 + j
+            half = all_ref.at[line, pl.ds(4 * (1 - c), 4)]
+            remote(half, half, s_send.at[index], s_recv.at[index], sibling).wait_recv()
+
+        @pl.when(step == 1 + 16 * later)
+        def _():
+            far_decays.wait_recv()
+            q_copy.wait_recv()
+            far = jnp.concatenate([far_ref[q] for q in range(4)], axis=0)
+            prepare(1, qr_ref, far * LOG2E)
 
         def group(rg, inner):
-            @pl.when((step == 0) & (rg == 1))
-            def _():
-                far_decays.wait_recv()
-                q_copy.wait_recv()
-                far = jnp.concatenate([far_ref[q] for q in range(4)], axis=0)
-                prepare(1, qr_ref, far * LOG2E)
-
             last = own_line + rg * (15 - 2 * own_line)
             tp_row = tp + rg * (7 - 2 * tp)
 
@@ -389,9 +403,12 @@
 
             return inner
 
-        return lax.fori_loop(0, 2, group, carry)
-
-    lax.fori_loop(0, 16, body, 0)
+        one = lambda test: test.astype(jnp.int32)
+        own_rows = one(line <= own_line) * one(step != 1) * (1 - again)
+        far_rows = one(line <= 15 - own_line) * ((1 - later) * one(step != 0) + again)
+        return lax.fori_loop(1 - own_rows, 1 + far_rows, group, carry)
+
+    lax.fori_loop(0, 17 + later * (16 - own_line), body, 0)
 
     def finish(rg, to_ref):
         inverse = 1.0 / jnp.sum(sum_ref[rg], axis=0, keepdims=True)
@@ -433,14 +450,19 @@
     back.wait_send()
 
 
-def main(norm, kv, d, qg, wq, wo, bounded):
+def main(x, in_gain, wk, wv, qg, kg, d, wq, wo, bounded):
     dma = lambda *n: pltpu.SemaphoreType.DMA(n)
     return pl.pallas_call(
-        functools.partial(main_kernel, bounded, 512 if bounded else 256),
-        out_shape=jax.ShapeDtypeStruct((128, 2048), bf),
-        in_specs=[VM, VM, VM, VM, HBM, HBM],
-        out_specs=VM,
+        functools.partial(main_kernel, bounded, 512),
+        out_shape=[jax.ShapeDtypeStruct((128, 2048), bf), jax.ShapeDtypeStruct((1,), f32)],
+        in_specs=[HBM, VM, HBM, HBM, VM, VM, VM, HBM, HBM],
+        out_specs=[VM, pl.BlockSpec(memory_space=pltpu.SMEM)],
         scratch_shapes=[
+            pltpu.VMEM((128, 2048), bf),
+            pltpu.VMEM((2048, 128), bf),
+            pltpu.VMEM((2048, 128), bf),
+            pltpu.VMEM((128, 2048), bf),
+            pltpu.VMEM((2, 128, 128), bf),
             pltpu.VMEM((16, 8, 152, 128), bf),
             pltpu.VMEM((4, 2, 1024), f32),
             pltpu.VMEM((4, 2, 128), f32),
@@ -457,7 +479,9 @@
             pltpu.VMEM((2, 8, 1024), f32),
             pltpu.VMEM((2, 8, 1024), f32),
             pltpu.VMEM((2, 8, 128), f32),
-            dma(3),
+            pltpu.VMEM((1024, 128), bf),
+            pltpu.VMEM((LAG + 1, ROWS, 512), bf),
+            dma(6),
             dma(4),
             dma(4),
             dma(4),
@@ -472,26 +496,27 @@
         compiler_params=pltpu.CompilerParams(
             collective_id=0 if bounded else 1,
             has_side_effects=True,
-            vmem_limit_bytes=60 * 1024 * 1024,
+            vmem_limit_bytes=67_000_000,
         ),
         name="main_bounded" if bounded else "main_any",
-    )(norm, kv, d, qg, wq, wo)
+    )(x, in_gain, wk, wv, qg, kg, d, wq, wo)
 
 
 def per_device(inputs, in_gain, w_query, w_key, w_value, query_gain, key_gain, decay_sums, w_out):
-    query_gain = query_gain.reshape(1, -1)
-    key_gain = key_gain.reshape(1, -1)
-    norm, kv, bound = start(inputs, in_gain.reshape(1, -1), w_key, w_value, query_gain, key_gain)
-    return lax.cond(
-        bound[0] <= 64.0,
-        lambda *a: main(*a, True),
-        lambda *a: main(*a, False),
-        norm,
-        kv,
+    args = (
+        inputs,
+        in_gain.reshape(1, -1),
+        w_key,
+        w_value,
+        query_gain.reshape(1, -1),
+        key_gain.reshape(1, -1),
         decay_sums.T,
-        query_gain,
         w_query,
         w_out,
+    )
+    result, bound = main(*args, True)
+    return lax.cond(
+        bound[0] <= 64.0, lambda kept, *a: kept, lambda kept, *a: main(*a, False)[0], result, *args
     )
 
 

time: 87.2 us -> 143 us (1.64); the launches traced: 87 us -> 140 us
  Pallas kernels: 85.5 us -> 137 us
    pallas_call x2, Pallas kernels: 85.5 us -> 137 us  [main(): pl.pallas_call(functools.partial(main_kernel, bounded, 512), out_shape=[j...]
where the time goes in v3:
time: 143 us; the launch traced here: 140 us
  Pallas kernels  137 us (96%)
  local copies, waits for them, and re-layouts  1.9 us (1%)
    pallas_call x2, Pallas kernels, main(): pl.pallas_call(functools.partial(main_kernel, bounded, 512), out_shape=[j...  137 us

profile of v3, /device:TPU:33, one launch (start us, length us, event | category | flops | bytes accessed | tf_op | source)
XLA Modules:
  0.0 140.1 jit_solution(9943784396138836433)
XLA Ops:
  0.0 0.0 copy-start
  0.0 0.0 copy-start.1
  0.0 0.0 copy-start.2
  0.0 0.0 copy-start.3
  0.0 54.3 %main_bounded.1 = (bf16[128,2048]{1,0:T(8,128)(2,1)}, f32[1]{0:T(128)}) custom-call(bf16[128,2048]{1,0:T(8,128)(2,1)} %refs_0_.1, f32[1,2048]{1,0:T(1,128)} %bitcast.5, bf16[2048,128]{1,0:T(8,128)(2,1)} %refs_2_.1, bf16[2048,128]{1,0:T(8,128)(2,1)} %refs_3_.1, f32[1,64]{1,0:T(1,128)} %bitcast.9, f32[1,64]{1,0:T(1,128)} %bitcast.11, f32[2,1024]{1,0:T(2,128)} %bitcast.7, ...), custom_call_target="tpu_custom_call" | custom-call | tf_op jit(solution)/shard_map/main_bounded/pallas_call | solution.py:455
  54.9 0.0 copy-done
  54.9 0.0 copy-done.1
  55.0 0.0 copy-done.2
  55.0 0.0 copy-done.3
  55.0 83.2 %conditional.1 = (bf16[128,2048]{1,0:T(8,128)(2,1)}) conditional(s32[]{:T(128)} %bitcast.4, (bf16[128,2048]{1,0:T(8,128)(2,1)}, f32[1,2048]{1,0:T(1,128)S(1)}, bf16[2048,128]{1,0:T(8,128)(2,1)}, bf16[2048,128]{1,0:T(8,128)(2,1)}, f32[1,64]{1,0:T(1,128)S(1)}, /*index=5*/f32[1,64]{1,0:T(1,128)S(1)}, f32[2,1024]{1,0:T(2,128)S(1)}, ...), branch_computations={%region_0.0_spmd, %region_1.0_spmd} | conditional | bytes 8 | solution.py:518
  55.0 83.2 %main_any.1 = (bf16[128,2048]{1,0:T(8,128)(2,1)}, f32[1]{0:T(128)}) custom-call(bf16[128,2048]{1,0:T(8,128)(2,1)} %get-tuple-element.27.refs_0_, f32[1,2048]{1,0:T(1,128)S(1)} %get-tuple-element.28.refs_1_, bf16[2048,128]{1,0:T(8,128)(2,1)} %get-tuple-element.29.refs_2_, bf16[2048,128]{1,0:T(8,128)(2,1)} %get-tuple-element.30.refs_3_, ...), custom_call_target="tpu_custom_call" | custom-call | tf_op jit(solution)/shard_map/cond/branch_0_fun/main_any/pallas_call | solution.py:455
  138.2 1.9 %copy.15 = bf16[128,2048]{1,0:T(8,128)(2,1)} copy(bf16[128,2048]{1,0:T(8,128)(2,1)} %get-tuple-element.41) | data formatting | bytes 1048576
Async XLA Ops:
  0.0 54.9 %copy-start = (f32[2048]{0:T(1024)S(1)}, f32[2048]{0:T(1024)}, u32[]{:S(2)}) copy-start(f32[2048]{0:T(1024)} %param.12) | copy-start | bytes 24580
  0.0 54.9 %copy-start.1 = (f32[1024,2]{0,1:T(2,128)S(1)}, f32[1024,2]{0,1:T(2,128)}, u32[]{:S(2)}) copy-start(f32[1024,2]{0,1:T(2,128)} %param.18) | copy-start | bytes 24580
  0.0 54.9 %copy-start.2 = (f32[64]{0:T(128)S(1)}, f32[64]{0:T(128)}, u32[]{:S(2)}) copy-start(f32[64]{0:T(128)} %param.16) | copy-start | bytes 772
  0.0 55.0 %copy-start.3 = (f32[64]{0:T(128)S(1)}, f32[64]{0:T(128)}, u32[]{:S(2)}) copy-start(f32[64]{0:T(128)} %param.17) | copy-start | bytes 772

commit v4 on v3

--- a/solution.py
+++ b/solution.py
@@ -30,18 +30,25 @@
 
 
 HBM = pl.BlockSpec(memory_space=pltpu.HBM)
-SEQ_J = (0, 3, 1, 0, 0, 2, 0, 3, 3, 1, 1, 3, 1, 2, 2, 2)
-SEQ_K = (0, 0, 0, 3, 1, 0, 2, 3, 1, 3, 1, 2, 2, 3, 1, 2)
+GROUPS = (
+    ((0, 0), (3, 0), (0, 3)),
+    ((1, 0), (0, 1)),
+    ((2, 0), (0, 2)),
+    ((3, 3), (1, 3)),
+    ((3, 1), (1, 1)),
+    ((3, 2), (1, 2), (2, 3), (2, 1)),
+    ((2, 2),),
+)
 ROWS, LAG = 256, 3
 
 
 def packed(values):
-    total = sum(v << 2 * i for i, v in enumerate(values))
+    total = sum(v << 4 * i for i, v in enumerate(values))
     return total - (1 << 32) if total >> 31 else total
 
 
 def unpacked(values, index):
-    return lax.shift_right_logical(jnp.int32(packed(values)), 2 * index) & 3
+    return lax.shift_right_logical(jnp.int32(packed(values)), 4 * index) & 15
 
 
 def column(row):
@@ -272,16 +279,25 @@
     if not bounded:
         max_ref[...] = jnp.full(max_ref.shape, -1e30, f32)
 
-    def attend(rg, line, tp_row, masked):
-        ref_d = refd_ref[rg]
-        for p in range(8):
-            ka_ref[p * 128 : (p + 1) * 128] = load_keys(all_ref, line, p, ref_d, ones)
-        units = [(m, n) for m in range(1024 // ROWS) for n in range(1024 // tile)]
+    def attend(parts, tp_row, masked):
+        for i, (rg, line) in enumerate(parts):
+            ref_d = refd_ref[rg]
+            for p in range(8):
+                first = i * 1024 + p * 128
+                ka_ref[first : first + 128] = load_keys(all_ref, line, p, ref_d, ones)
+        units = [
+            (i, m, n)
+            for i in range(len(parts))
+            for m in range(1024 // ROWS)
+            for n in range(1024 // tile)
+        ]
 
         def weigh(u):
-            m, n = units[u]
+            i, m, n = units[u]
+            rg = parts[i][0]
             cols = slice(n * tile, (n + 1) * tile)
-            keys = ka_ref[m * ROWS : (m + 1) * ROWS]
+            first = i * 1024 + m * ROWS
+            keys = ka_ref[first : first + ROWS]
             scores = jnp.dot(keys, qa_ref[rg, :, cols], preferred_element_type=f32)
             if masked:
                 shape = (ROWS, tile)
@@ -303,7 +319,8 @@
             wt_ref[u % (lag + 1)] = weights.astype(bf)
 
         def gather_values(u):
-            m, n = units[u]
+            i, m, n = units[u]
+            rg, line = parts[i]
             cols = slice(n * tile, (n + 1) * tile)
             first = m * ROWS // 128
             values = jnp.concatenate(
@@ -320,33 +337,65 @@
             if u >= lag:
                 gather_values(u - lag)
 
+    def got(step, slot):
+        ring(step, slot).wait_recv()
+
+    def pass_on(step, sub):
+        for slot in (sub, 2 + sub):
+            ring(step, slot).start()
+
     def act_1():
-        ring_relay(0)
+        got(0, 0)
+        ring(0, 4).start()
+        pass_on(4, 0)
+        got(0, 2)
+        pass_on(2, 0)
+        got(1, 0)
+        ring(1, 4).start()
+        got(0, 3)
+        ring(0, 5).start()
+        pass_on(2, 1)
+        got(0, 1)
+        pass_on(4, 1)
         share(3, 0).start()
         share(1, 0).start()
-        ring_relay(1)
+        got(1, 3)
+        ring(1, 5).start()
+        got(1, 1)
+        got(1, 2)
+        share(0, 3).start()
+        share(0, 1).start()
+
+    def act_3():
+        got(0, 4)
+        pass_on(3, 0)
+        got(0, 5)
+        pass_on(3, 1)
+        share(2, 0).start()
+        ring_end(1)
+        share(0, 2).start()
+
+    def act_6():
+        got(4, 0)
+        ring(4, 4).start()
+        got(2, 0)
+        ring(2, 4).start()
+        got(2, 3)
+        ring(2, 5).start()
+        got(2, 1)
+        got(2, 2)
+        share(1, 3).start()
+        share(1, 1).start()
+        got(4, 3)
+        ring(4, 5).start()
+        got(4, 1)
+        got(4, 2)
+        share(3, 3).start()
+        share(3, 1).start()
 
         @pl.when(late)
         def _():
             q_copy.start()
-
-        ring_start(4)
-        ring_start(2)
-        share(0, 3).start()
-        share(0, 1).start()
-
-    def act_3():
-        ring_end(0)
-        ring_start(3)
-        share(2, 0).start()
-        ring_end(1)
-        share(0, 2).start()
-
-    def act_6():
-        for j in (3, 1):
-            ring_relay(1 + j)
-            share(j, 3).start()
-            share(j, 1).start()
 
     def act_9():
         ring_relay(3)
@@ -360,66 +409,123 @@
         ring_end(3)
         share(2, 2).start()
 
-    actions = {1: act_1, 4: act_3, 7: act_6, 10: act_9, 14: act_13}
-
     later = jnp.where(late, 0, 1)
-
-    def body(step, carry):
-        for at, action in actions.items():
-
-            @pl.when(step == at)
+    one = lambda test: test.astype(jnp.int32)
+
+    def wait_half(j, k):
+        half = all_ref.at[line_at(j, k), pl.ds(4 * (1 - c), 4)]
+        index = k * 4 + j
+        remote(half, half, s_send.at[index], s_recv.at[index], sibling).wait_recv()
+
+    far_line = 15 - own_line
+    last_line = line_at(2, 2)
+    early = jnp.logical_not(late) & (last_line > far_line)
+
+    def back(part):
+        rows = pl.ds(part * 256, 256)
+        return remote(
+            os_ref.at[rows], got_ref.at[rows], x_send.at[2 + part], x_recv.at[2 + part], mirror
+        )
+
+    def finish(rg, to_ref):
+        inverse = 1.0 / jnp.sum(sum_ref[rg], axis=0, keepdims=True)
+        for h in range(8):
+            cols = slice(h * 128, (h + 1) * 128)
+            to_ref[h * 64 : (h + 1) * 64, :] = (acc_ref[rg, :, cols] * inverse[:, cols]).astype(bf)
+
+    wait_half(0, 0)
+    attend([(0, own_line)], tp, True)
+
+    def body(group, carry):
+        actions = ((0, act_1), (1 + later, act_3), (2 + later, act_6), (4, act_9), (6 + later, act_13))
+        for at, action in actions:
+
+            @pl.when(group == at)
             def _(action=action):
                 action()
 
-        place = jnp.maximum(step - 1, 0) & 15
-        j, k = unpacked(SEQ_J, place), unpacked(SEQ_K, place)
-        again = (step >= 17).astype(jnp.int32)
-        line = line_at(j, k) * (1 - again) + (step - 17) * again
-
-        @pl.when((step != 1) & (step < 17))
+        @pl.when((group == 6) & early)
         def _():
-            index = k * 4 + j
-            half = all_ref.at[line, pl.ds(4 * (1 - c), 4)]
-            remote(half, half, s_send.at[index], s_recv.at[index], sibling).wait_recv()
-
-        @pl.when(step == 1 + 16 * later)
+            for part in range(2):
+                back(part).start()
+
+        for at, members in enumerate(GROUPS):
+
+            @pl.when(group == (at + later if at == 6 else at))
+            def _(members=members):
+                for j, k in members:
+                    if (j, k) != (0, 0):
+                        wait_half(j, k)
+
+        @pl.when(group == 5 * later)
         def _():
             far_decays.wait_recv()
             q_copy.wait_recv()
             far = jnp.concatenate([far_ref[q] for q in range(4)], axis=0)
             prepare(1, qr_ref, far * LOG2E)
 
-        def group(rg, inner):
-            last = own_line + rg * (15 - 2 * own_line)
-            tp_row = tp + rg * (7 - 2 * tp)
-
-            @pl.when(line < last)
-            def _():
-                attend(rg, line, tp_row, False)
-
-            @pl.when(line == last)
-            def _():
-                attend(rg, line, tp_row, True)
-
+        turn = group + later * (2 * one(group == 5) - one(group > 5))
+        again = one(turn == 7)
+        size = unpacked((3, 2, 2, 2, 2, 4, 1, 0), turn)
+        lines = []
+        for i in range(4):
+            pick = lambda axis: unpacked(
+                [g[i][axis] if i < len(g) else 0 for g in GROUPS] + [0], turn
+            )
+            lines.append(line_at(pick(0), pick(1)))
+        flags = []
+        for i in range(4):
+            here = one(i < size)
+            flags.append(here * one(lines[i] < own_line))
+            flags.append(here * one(lines[i] < far_line) * jnp.where(turn == 6, 1, 1 - later))
+        before, count = [], 0
+        for flag in flags:
+            before.append(count)
+            count = count + flag
+        count = count * (1 - again) + (far_line - one(last_line < far_line)) * again
+
+        def unit(index):
+            rg, line = again, (index + one(index >= last_line)) * again
+            for i in range(8):
+                chosen = flags[i] * one(before[i] == index)
+                line = line + chosen * lines[i // 2]
+                if i % 2:
+                    rg = rg + chosen
+            return rg, line
+
+        def pair(index, inner):
+            attend([unit(2 * index), unit(2 * index + 1)], tp, False)
             return inner
 
-        one = lambda test: test.astype(jnp.int32)
-        own_rows = one(line <= own_line) * one(step != 1) * (1 - again)
-        far_rows = one(line <= 15 - own_line) * ((1 - later) * one(step != 0) + again)
-        return lax.fori_loop(1 - own_rows, 1 + far_rows, group, carry)
-
-    lax.fori_loop(0, 17 + later * (16 - own_line), body, 0)
-
-    def finish(rg, to_ref):
-        inverse = 1.0 / jnp.sum(sum_ref[rg], axis=0, keepdims=True)
-        for h in range(8):
-            cols = slice(h * 128, (h + 1) * 128)
-            to_ref[h * 64 : (h + 1) * 64, :] = (acc_ref[rg, :, cols] * inverse[:, cols]).astype(bf)
-
-    finish(1, os_ref)
+        lax.fori_loop(0, count // 2, pair, 0)
+
+        @pl.when((count & 1) == 1)
+        def _():
+            attend([unit(count - 1)], tp, False)
+
+        @pl.when(group == 4 + later)
+        def _():
+            attend([(1, far_line)], 7 - tp, True)
+
+        @pl.when((group == 5) & early)
+        def _():
+            finish(1, os_ref)
+
+        return carry
+
+    lax.fori_loop(0, 7 + later, body, 0)
+
+    @pl.when(jnp.logical_not(early))
+    def _():
+        finish(1, os_ref)
+
     finish(0, near_ref)
-    back = remote(os_ref, got_ref, x_send.at[2], x_recv.at[2], mirror)
-    back.start()
+
+    @pl.when(jnp.logical_not(early))
+    def _():
+        for part in range(2):
+            back(part).start()
+
     out_copy.wait()
     near = near_ref[...].T
     for n in range(4):
@@ -441,13 +547,19 @@
     for j in range(4):
         for k in range(4):
             share(j, k).wait_send()
-    back.wait_recv()
-    far = got_ref[...].T
-    for n in range(4):
-        cols = slice(n * 512, (n + 1) * 512)
-        rest = jnp.dot(far, wo_ref[pl.ds(w_far, 512), cols], preferred_element_type=f32)
-        out_ref[:, cols] = (part_ref[:, cols] + rest).astype(bf)
-    back.wait_send()
+    for part in range(2):
+        back(part).wait_recv()
+        far = got_ref[part * 256 : (part + 1) * 256, :].T
+        rows = pl.ds(pl.multiple_of(w_far + part * 256, 256), 256)
+        for n in range(2):
+            cols = slice(n * 1024, (n + 1) * 1024)
+            rest = jnp.dot(far, wo_ref[rows, cols], preferred_element_type=f32)
+            if part == 0:
+                part_ref[:, cols] += rest
+            else:
+                out_ref[:, cols] = (part_ref[:, cols] + rest).astype(bf)
+    for part in range(2):
+        back(part).wait_send()
 
 
 def main(x, in_gain, wk, wv, qg, kg, d, wq, wo, bounded):
@@ -479,15 +591,15 @@
             pltpu.VMEM((2, 8, 1024), f32),
             pltpu.VMEM((2, 8, 1024), f32),
             pltpu.VMEM((2, 8, 128), f32),
-            pltpu.VMEM((1024, 128), bf),
+            pltpu.VMEM((2048, 128), bf),
             pltpu.VMEM((LAG + 1, ROWS, 512), bf),
             dma(6),
             dma(4),
             dma(4),
             dma(4),
             dma(4),
-            dma(3),
-            dma(3),
+            dma(4),
+            dma(4),
             dma(30),
             dma(30),
             dma(16),

time: 143 us -> 137 us (0.958)
  the two profiles are of different devices: /device:TPU:33 before, /device:TPU:59 now
where the time goes in v4:
time: 137 us
  Pallas kernels  134 us (98%)
  local copies, waits for them, and re-layouts  1.9 us (1%)
    pallas_call x2, Pallas kernels, main(): pl.pallas_call(functools.partial(main_kernel, bounded, 512), out_shape=[j...  134 us

profile of v4, /device:TPU:59, one launch (start us, length us, event | category | flops | bytes accessed | tf_op | source)
XLA Modules:
  0.0 136.5 jit_solution(17896304167209661226)
XLA Ops:
  0.0 0.0 copy-start
  0.0 0.0 copy-start.1
  0.0 0.0 copy-start.2
  0.0 0.0 copy-start.3
  0.0 51.6 %main_bounded.1 = (bf16[128,2048]{1,0:T(8,128)(2,1)}, f32[1]{0:T(128)}) custom-call(bf16[128,2048]{1,0:T(8,128)(2,1)} %refs_0_.1, f32[1,2048]{1,0:T(1,128)} %bitcast.5, bf16[2048,128]{1,0:T(8,128)(2,1)} %refs_2_.1, bf16[2048,128]{1,0:T(8,128)(2,1)} %refs_3_.1, f32[1,64]{1,0:T(1,128)} %bitcast.9, f32[1,64]{1,0:T(1,128)} %bitcast.11, f32[2,1024]{1,0:T(2,128)} %bitcast.7, ...), custom_call_target="tpu_custom_call" | custom-call | tf_op jit(solution)/shard_map/main_bounded/pallas_call | solution.py:567
  52.3 0.0 copy-done
  52.3 0.0 copy-done.1
  52.3 0.0 copy-done.2
  52.3 0.0 copy-done.3
  52.3 82.3 %conditional.1 = (bf16[128,2048]{1,0:T(8,128)(2,1)}) conditional(s32[]{:T(128)} %bitcast.4, (bf16[128,2048]{1,0:T(8,128)(2,1)}, f32[1,2048]{1,0:T(1,128)S(1)}, bf16[2048,128]{1,0:T(8,128)(2,1)}, bf16[2048,128]{1,0:T(8,128)(2,1)}, f32[1,64]{1,0:T(1,128)S(1)}, /*index=5*/f32[1,64]{1,0:T(1,128)S(1)}, f32[2,1024]{1,0:T(2,128)S(1)}, ...), branch_computations={%region_0.0_spmd, %region_1.0_spmd} | conditional | bytes 8 | solution.py:630
  52.3 82.1 %main_any.1 = (bf16[128,2048]{1,0:T(8,128)(2,1)}, f32[1]{0:T(128)}) custom-call(bf16[128,2048]{1,0:T(8,128)(2,1)} %get-tuple-element.27.refs_0_, f32[1,2048]{1,0:T(1,128)S(1)} %get-tuple-element.28.refs_1_, bf16[2048,128]{1,0:T(8,128)(2,1)} %get-tuple-element.29.refs_2_, bf16[2048,128]{1,0:T(8,128)(2,1)} %get-tuple-element.30.refs_3_, ...), custom_call_target="tpu_custom_call" | custom-call | tf_op jit(solution)/shard_map/cond/branch_0_fun/main_any/pallas_call | solution.py:567
  134.6 1.9 %copy.15 = bf16[128,2048]{1,0:T(8,128)(2,1)} copy(bf16[128,2048]{1,0:T(8,128)(2,1)} %get-tuple-element.41) | data formatting | bytes 1048576
Async XLA Ops:
  0.0 52.3 %copy-start = (f32[2048]{0:T(1024)S(1)}, f32[2048]{0:T(1024)}, u32[]{:S(2)}) copy-start(f32[2048]{0:T(1024)} %param.12) | copy-start | bytes 24580
  0.0 52.3 %copy-start.1 = (f32[1024,2]{0,1:T(2,128)S(1)}, f32[1024,2]{0,1:T(2,128)}, u32[]{:S(2)}) copy-start(f32[1024,2]{0,1:T(2,128)} %param.18) | copy-start | bytes 24580
  0.0 52.3 %copy-start.2 = (f32[64]{0:T(128)S(1)}, f32[64]{0:T(128)}, u32[]{:S(2)}) copy-start(f32[64]{0:T(128)} %param.16) | copy-start | bytes 772
  0.0 52.3 %copy-start.3 = (f32[64]{0:T(128)S(1)}, f32[64]{0:T(128)}, u32[]{:S(2)}) copy-start(f32[64]{0:T(128)} %param.17) | copy-start | bytes 772

commit v5 on v4

--- a/solution.py
+++ b/solution.py
@@ -420,6 +420,7 @@
     far_line = 15 - own_line
     last_line = line_at(2, 2)
     early = jnp.logical_not(late) & (last_line > far_line)
+    hold = jnp.logical_not(late) & (last_line <= far_line)
 
     def back(part):
         rows = pl.ds(part * 256, 256)
@@ -437,21 +438,21 @@
     attend([(0, own_line)], tp, True)
 
     def body(group, carry):
-        actions = ((0, act_1), (1 + later, act_3), (2 + later, act_6), (4, act_9), (6 + later, act_13))
+        actions = ((0, act_1), (1 + later, act_3), (2 + later, act_6), (4, act_9), (6 + one(early), act_13))
         for at, action in actions:
 
             @pl.when(group == at)
             def _(action=action):
                 action()
 
-        @pl.when((group == 6) & early)
+        @pl.when(group == jnp.where(late, 99, 6 + one(hold)))
         def _():
             for part in range(2):
                 back(part).start()
 
         for at, members in enumerate(GROUPS):
 
-            @pl.when(group == (at + later if at == 6 else at))
+            @pl.when(group == (at + one(early) if at == 6 else at))
             def _(members=members):
                 for j, k in members:
                     if (j, k) != (0, 0):
@@ -464,7 +465,8 @@
             far = jnp.concatenate([far_ref[q] for q in range(4)], axis=0)
             prepare(1, qr_ref, far * LOG2E)
 
-        turn = group + later * (2 * one(group == 5) - one(group > 5))
+        turn = group + later * (2 * one(group == 5) - one(group > 5) * one(early))
+        turn = turn - 2 * one(hold) * one(group == 7)
         again = one(turn == 7)
         size = unpacked((3, 2, 2, 2, 2, 4, 1, 0), turn)
         lines = []
@@ -476,8 +478,10 @@
         flags = []
         for i in range(4):
             here = one(i < size)
-            flags.append(here * one(lines[i] < own_line))
+            flags.append(here * one(lines[i] < own_line) * (1 - one(hold) * one(group == 6)))
             flags.append(here * one(lines[i] < far_line) * jnp.where(turn == 6, 1, 1 - later))
+        lines.append(last_line)
+        flags.append(one(last_line < own_line) * one(hold) * one(group == 7))
         before, count = [], 0
         for flag in flags:
             before.append(count)
@@ -486,7 +490,7 @@
 
         def unit(index):
             rg, line = again, (index + one(index >= last_line)) * again
-            for i in range(8):
+            for i in range(9):
                 chosen = flags[i] * one(before[i] == index)
                 line = line + chosen * lines[i // 2]
                 if i % 2:
@@ -507,7 +511,7 @@
         def _():
             attend([(1, far_line)], 7 - tp, True)
 
-        @pl.when((group == 5) & early)
+        @pl.when(group == jnp.where(late, 99, 5 + one(hold)))
         def _():
             finish(1, os_ref)
 
@@ -515,13 +519,13 @@
 
     lax.fori_loop(0, 7 + later, body, 0)
 
-    @pl.when(jnp.logical_not(early))
+    @pl.when(late)
     def _():
         finish(1, os_ref)
 
     finish(0, near_ref)
 
-    @pl.when(jnp.logical_not(early))
+    @pl.when(late)
     def _():
         for part in range(2):
             back(part).start()
@@ -608,7 +612,7 @@
         compiler_params=pltpu.CompilerParams(
             collective_id=0 if bounded else 1,
             has_side_effects=True,
-            vmem_limit_bytes=67_000_000,
+            vmem_limit_bytes=60 * 1024 * 1024,
         ),
         name="main_bounded" if bounded else "main_any",
     )(x, in_gain, wk, wv, qg, kg, d, wq, wo)

time: 137 us -> 128 us (0.934)
  the two profiles are of different devices: /device:TPU:59 before, /device:TPU:65 now
where the time goes in v5:
time: 128 us; the launch traced here: 127 us
  Pallas kernels  126 us (98%)
    pallas_call x2, Pallas kernels, main(): pl.pallas_call(functools.partial(main_kernel, bounded, 512), out_shape=[j...  126 us

profile of v5, /device:TPU:65, one launch (start us, length us, event | category | flops | bytes accessed | tf_op | source)
XLA Modules:
  0.0 127.5 jit_solution(8892683766287101763)
XLA Ops:
  0.0 0.0 copy-start
  0.0 0.0 copy-start.1
  0.0 0.0 copy-start.2
  0.0 0.0 copy-start.3
  0.0 0.0 copy-start.4
  0.0 0.0 copy-start.5
  0.0 0.0 copy-start.6
  0.0 47.6 %main_bounded.1 = (bf16[128,2048]{1,0:T(8,128)(2,1)S(1)}, f32[1]{0:T(128)}) custom-call(bf16[128,2048]{1,0:T(8,128)(2,1)} %refs_0_.1, f32[1,2048]{1,0:T(1,128)} %bitcast.5, bf16[2048,128]{1,0:T(8,128)(2,1)} %refs_2_.1, bf16[2048,128]{1,0:T(8,128)(2,1)} %refs_3_.1, f32[1,64]{1,0:T(1,128)} %bitcast.9, f32[1,64]{1,0:T(1,128)} %bitcast.11, f32[2,1024]{1,0:T(2,128)} %bitcast.7, ...), custom_call_target="tpu_custom_call" | custom-call | tf_op jit(solution)/shard_map/main_bounded/pallas_call | solution.py:571
  48.3 0.0 copy-done
  48.3 0.0 copy-done.1
  48.3 0.0 copy-done.2
  48.3 0.0 copy-done.3
  48.3 0.0 copy-done.4
  48.3 0.0 copy-done.5
  48.3 0.0 copy-done.6
  48.3 78.3 %conditional.1 = (bf16[128,2048]{1,0:T(8,128)(2,1)S(1)}) conditional(s32[]{:T(128)} %bitcast.4, (bf16[128,2048]{1,0:T(8,128)(2,1)S(1)}, f32[1,2048]{1,0:T(1,128)S(1)}, bf16[2048,128]{1,0:T(8,128)(2,1)S(1)}, bf16[2048,128]{1,0:T(8,128)(2,1)S(1)}, f32[1,64]{1,0:T(1,128)S(1)}, /*index=5*/f32[1,64]{1,0:T(1,128)S(1)}, f32[2,1024]{1,0:T(2,128)S(1)}, ...), branch_computations={%region_0.0_spmd, %region_1.0_spmd} | conditional | bytes 8 | solution.py:634
  48.3 78.1 %main_any.1 = (bf16[128,2048]{1,0:T(8,128)(2,1)S(1)}, f32[1]{0:T(128)}) custom-call(bf16[128,2048]{1,0:T(8,128)(2,1)S(1)} %get-tuple-element.27.refs_0_, f32[1,2048]{1,0:T(1,128)S(1)} %get-tuple-element.28.refs_1_, bf16[2048,128]{1,0:T(8,128)(2,1)S(1)} %get-tuple-element.29.refs_2_, bf16[2048,128]{1,0:T(8,128)(2,1)S(1)} %get-tuple-element.30.refs_3_, ...), custom_call_target="tpu_custom_call" | custom-call | tf_op jit(solution)/shard_map/cond/branch_0_fun/main_any/pallas_call | solution.py:571
  126.7 0.8 copy.15
Async XLA Ops:
  0.0 48.3 %copy-start = (bf16[128,2048]{1,0:T(8,128)(2,1)S(1)}, bf16[128,2048]{1,0:T(8,128)(2,1)}, u32[]{:S(2)}) copy-start(bf16[128,2048]{1,0:T(8,128)(2,1)} %refs_0_.1) | copy-start | bytes 1572868
  0.0 48.3 %copy-start.1 = (bf16[2048,128]{1,0:T(8,128)(2,1)S(1)}, bf16[2048,128]{1,0:T(8,128)(2,1)}, u32[]{:S(2)}) copy-start(bf16[2048,128]{1,0:T(8,128)(2,1)} %refs_2_.1) | copy-start | bytes 1572868
  0.0 48.3 %copy-start.2 = (bf16[2048,128]{1,0:T(8,128)(2,1)S(1)}, bf16[2048,128]{1,0:T(8,128)(2,1)}, u32[]{:S(2)}) copy-start(bf16[2048,128]{1,0:T(8,128)(2,1)} %refs_3_.1) | copy-start | bytes 1572868
  0.0 48.3 %copy-start.3 = (f32[2048]{0:T(1024)S(1)}, f32[2048]{0:T(1024)}, u32[]{:S(2)}) copy-start(f32[2048]{0:T(1024)} %param.12) | copy-start | bytes 24580
  0.0 48.3 %copy-start.4 = (f32[1024,2]{0,1:T(2,128)S(1)}, f32[1024,2]{0,1:T(2,128)}, u32[]{:S(2)}) copy-start(f32[1024,2]{0,1:T(2,128)} %param.18) | copy-start | bytes 24580
  0.0 48.3 %copy-start.5 = (f32[64]{0:T(128)S(1)}, f32[64]{0:T(128)}, u32[]{:S(2)}) copy-start(f32[64]{0:T(128)} %param.16) | copy-start | bytes 772
  0.0 48.3 %copy-start.6 = (f32[64]{0:T(128)S(1)}, f32[64]{0:T(128)}, u32[]{:S(2)}) copy-start(f32[64]{0:T(128)} %param.17) | copy-start | bytes 772

commit v6 on v5

--- a/solution.py
+++ b/solution.py
@@ -438,7 +438,7 @@
     attend([(0, own_line)], tp, True)
 
     def body(group, carry):
-        actions = ((0, act_1), (1 + later, act_3), (2 + later, act_6), (4, act_9), (6 + one(early), act_13))
+        actions = ((0, act_1), (1 + later, act_3), (2 + later, act_6), (5, act_9), (6 + one(early), act_13))
         for at, action in actions:
 
             @pl.when(group == at)

time: 128 us -> 127 us (level)
  the two profiles are of different devices: /device:TPU:65 before, /device:TPU:67 now
where the time goes in v6:
time: 127 us
  Pallas kernels  125 us (98%)
    pallas_call x2, Pallas kernels, main(): pl.pallas_call(functools.partial(main_kernel, bounded, 512), out_shape=[j...  125 us

profile of v6, /device:TPU:67, one launch (start us, length us, event | category | flops | bytes accessed | tf_op | source)
XLA Modules:
  0.0 127.1 jit_solution(16335256024170041721)
XLA Ops:
  0.0 0.0 copy-start
  0.0 0.0 copy-start.1
  0.0 0.0 copy-start.2
  0.0 0.0 copy-start.3
  0.0 0.0 copy-start.4
  0.0 0.0 copy-start.5
  0.0 0.0 copy-start.6
  0.0 46.6 %main_bounded.1 = (bf16[128,2048]{1,0:T(8,128)(2,1)S(1)}, f32[1]{0:T(128)}) custom-call(bf16[128,2048]{1,0:T(8,128)(2,1)} %refs_0_.1, f32[1,2048]{1,0:T(1,128)} %bitcast.5, bf16[2048,128]{1,0:T(8,128)(2,1)} %refs_2_.1, bf16[2048,128]{1,0:T(8,128)(2,1)} %refs_3_.1, f32[1,64]{1,0:T(1,128)} %bitcast.9, f32[1,64]{1,0:T(1,128)} %bitcast.11, f32[2,1024]{1,0:T(2,128)} %bitcast.7, ...), custom_call_target="tpu_custom_call" | custom-call | tf_op jit(solution)/shard_map/main_bounded/pallas_call | solution.py:571
  47.2 0.0 copy-done
  47.3 0.0 copy-done.1
  47.3 0.0 copy-done.2
  47.3 0.0 copy-done.3
  47.3 0.0 copy-done.4
  47.3 0.0 copy-done.5
  47.3 0.0 copy-done.6
  47.3 79.0 %conditional.1 = (bf16[128,2048]{1,0:T(8,128)(2,1)S(1)}) conditional(s32[]{:T(128)} %bitcast.4, (bf16[128,2048]{1,0:T(8,128)(2,1)S(1)}, f32[1,2048]{1,0:T(1,128)S(1)}, bf16[2048,128]{1,0:T(8,128)(2,1)S(1)}, bf16[2048,128]{1,0:T(8,128)(2,1)S(1)}, f32[1,64]{1,0:T(1,128)S(1)}, /*index=5*/f32[1,64]{1,0:T(1,128)S(1)}, f32[2,1024]{1,0:T(2,128)S(1)}, ...), branch_computations={%region_0.0_spmd, %region_1.0_spmd} | conditional | bytes 8 | solution.py:634
  47.3 78.7 %main_any.1 = (bf16[128,2048]{1,0:T(8,128)(2,1)S(1)}, f32[1]{0:T(128)}) custom-call(bf16[128,2048]{1,0:T(8,128)(2,1)S(1)} %get-tuple-element.27.refs_0_, f32[1,2048]{1,0:T(1,128)S(1)} %get-tuple-element.28.refs_1_, bf16[2048,128]{1,0:T(8,128)(2,1)S(1)} %get-tuple-element.29.refs_2_, bf16[2048,128]{1,0:T(8,128)(2,1)S(1)} %get-tuple-element.30.refs_3_, ...), custom_call_target="tpu_custom_call" | custom-call | tf_op jit(solution)/shard_map/cond/branch_0_fun/main_any/pallas_call | solution.py:571
  126.3 0.8 copy.15
Async XLA Ops:
  0.0 47.2 %copy-start = (bf16[128,2048]{1,0:T(8,128)(2,1)S(1)}, bf16[128,2048]{1,0:T(8,128)(2,1)}, u32[]{:S(2)}) copy-start(bf16[128,2048]{1,0:T(8,128)(2,1)} %refs_0_.1) | copy-start | bytes 1572868
  0.0 47.3 %copy-start.1 = (bf16[2048,128]{1,0:T(8,128)(2,1)S(1)}, bf16[2048,128]{1,0:T(8,128)(2,1)}, u32[]{:S(2)}) copy-start(bf16[2048,128]{1,0:T(8,128)(2,1)} %refs_2_.1) | copy-start | bytes 1572868
  0.0 47.3 %copy-start.2 = (bf16[2048,128]{1,0:T(8,128)(2,1)S(1)}, bf16[2048,128]{1,0:T(8,128)(2,1)}, u32[]{:S(2)}) copy-start(bf16[2048,128]{1,0:T(8,128)(2,1)} %refs_3_.1) | copy-start | bytes 1572868
  0.0 47.3 %copy-start.3 = (f32[2048]{0:T(1024)S(1)}, f32[2048]{0:T(1024)}, u32[]{:S(2)}) copy-start(f32[2048]{0:T(1024)} %param.12) | copy-start | bytes 24580
  0.0 47.3 %copy-start.4 = (f32[1024,2]{0,1:T(2,128)S(1)}, f32[1024,2]{0,1:T(2,128)}, u32[]{:S(2)}) copy-start(f32[1024,2]{0,1:T(2,128)} %param.18) | copy-start | bytes 24580
  0.0 47.3 %copy-start.5 = (f32[64]{0:T(128)S(1)}, f32[64]{0:T(128)}, u32[]{:S(2)}) copy-start(f32[64]{0:T(128)} %param.16) | copy-start | bytes 772
  0.0 47.3 %copy-start.6 = (f32[64]{0:T(128)S(1)}, f32[64]{0:T(128)}, u32[]{:S(2)}) copy-start(f32[64]{0:T(128)} %param.17) | copy-start | bytes 772
